TPU v7x, 256 devices: a whole 4x4x8 slice. The times are simulated.
256 devices in a mesh: kv: 32 (over z, x), tp: 8 (over y, core).
Axes of the slice: x: 4, y: 4, z: 8, core: 2. Of those that a mesh axis runs over, the one named last changes fastest.
Arguments:
- tokens: bfloat16 [256, 12, 4096], P(None, None, 'kv'), may hold values from -6 to 6
- parents: int32 [256, 12], P('kv'), may hold values from -1 to 10, as said below
- accepted: int32 [256], P('kv'), may hold values from 0 to 6
- state: float32 [256, 64, 64, 128], P('kv', 'tp'), may hold values from -4 to 4
- conv_x: bfloat16 [256, 3, 4096], P('kv', None, 'tp'), may hold values from -6 to 6
- conv_b: bfloat16 [256, 3, 2048], P('kv', None, 'tp'), may hold values from -6 to 6
- conv_c: bfloat16 [256, 3, 2048], P('kv', None, 'tp'), may hold values from -6 to 6
- path_x: bfloat16 [256, 6, 4096], P('kv', None, 'tp'), may hold values from -6 to 6
- path_b: bfloat16 [256, 6, 2048], P('kv', None, 'tp'), may hold values from -6 to 6
- path_c: bfloat16 [256, 6, 2048], P('kv', None, 'tp'), may hold values from -6 to 6
- path_dt: bfloat16 [256, 6, 64], P('kv', None, 'tp'), may hold values from -6 to 6
- gain_in: float32 [4096], replicated, may hold values from 0.1 to 1.9
- w_x: bfloat16 [4096, 4096], P('kv', 'tp'), may hold values from -0.09375 to 0.09375
- w_z: bfloat16 [4096, 4096], P('kv', 'tp'), may hold values from -0.09375 to 0.09375
- w_b: bfloat16 [4096, 2048], P('kv', 'tp'), may hold values from -0.09375 to 0.09375
- w_c: bfloat16 [4096, 2048], P('kv', 'tp'), may hold values from -0.09375 to 0.09375
- w_dt: bfloat16 [4096, 64], replicated, may hold values from -0.09375 to 0.09375
- dt_bias: float32 [64], P('tp'), may hold values from -2 to 1
- a_log: float32 [64], P('tp'), may hold values from -3 to 1.5
- d_skip: float32 [64], P('tp'), may hold values from 0.5 to 1.5
- conv_wx: bfloat16 [4, 4096], P(None, 'tp'), may hold values from -3 to 3
- conv_wb: bfloat16 [4, 2048], P(None, 'tp'), may hold values from -3 to 3
- conv_wc: bfloat16 [4, 2048], P(None, 'tp'), may hold values from -3 to 3
- gain_out: float32 [4096], P('tp'), may hold values from 0.1 to 1.9
- w_out: bfloat16 [4096, 4096], P('tp', 'kv'), may hold values from -0.09375 to 0.09375
Outputs:
- mixed: bfloat16 [256, 12, 4096], P('kv', None, 'tp')
- new_state: float32 [256, 64, 64, 128], P('kv', 'tp')
Inputs may be any that keep to these rules, and one draw needn't show every extreme that they name: `parents`: each proposal's parent is -1 or an earlier proposal of the same sequence; the first proposal's parent is -1.
All inputs are finite; a program needn't handle non-finite values.
Results may differ from a plain program's by a relative error of at most 0.03.
Values may be sent and summed in bfloat16 or wider, within the bound.
A program may use at most 128 MiB of HBM per device.

v0:
```python
import jax
import jax.numpy as jnp
from jax import lax
from jax.sharding import Mesh
from jax.sharding import PartitionSpec as P

HPG = 4
KV = ("kv_0", "kv_1")


EPS = 1e-06
HIGH = lax.Precision.HIGHEST


def in_blocks(x, dim, length):
    dims = x.shape
    blocks = x.reshape(*dims[:dim], length, dims[dim] // length, *dims[dim + 1 :])
    return jnp.moveaxis(blocks, dim, 0)


def laid_out(blocks, dim):
    blocks = jnp.moveaxis(blocks, 0, dim)
    dims = blocks.shape
    return blocks.reshape(*dims[:dim], dims[dim] * dims[dim + 1], *dims[dim + 2 :])


def turned_blocks(blocks, axes, order):
    inside = blocks.shape[1:]
    out = blocks.reshape(*(lax.axis_size(a) for a in axes), *inside)
    for k in order:
        out = lax.all_to_all(out, axes[k], k, k, tiled=True)
    return out.reshape(-1, *inside)


def exchange_by_axis(x, axes, order, split_dim, concat_dim):
    blocks = in_blocks(x, split_dim, lax.axis_size(axes))
    return laid_out(turned_blocks(blocks, axes, order), concat_dim)


def sent_together(arrays, axis, dim, along):
    ends, at = ([], 0)
    for a in arrays[:-1]:
        at += a.shape[along]
        ends.append(at)
    both = jnp.concatenate(arrays, axis=along)
    return tuple(jnp.split(lax.all_gather(both, axis, axis=dim, tiled=True), ends, axis=along))


def whole_of(x, axes, dim):
    for axis in reversed(axes):
        x = lax.all_gather(x, axis, axis=dim, tiled=True)
    return x


def sum_at_owner(x, axis, dim):
    blocks = in_blocks(x, dim, lax.axis_size(axis))
    arrived = lax.all_to_all(blocks, axis, split_axis=0, concat_axis=0, tiled=True)
    return arrived.astype(jnp.float32).sum(axis=0)


def conv_window(history, taps, amount):
    values = history.astype(jnp.float32)
    weights = taps.astype(jnp.float32)
    summed = weights[0] * values[:, 0:amount, :]
    for distance in range(1, weights.shape[0]):
        summed = summed + weights[distance] * values[:, distance : distance + amount, :]
    return jax.nn.silu(summed)


def commit_rows(history, accepted, keep):
    picked = accepted[:, None] + jnp.arange(keep, dtype=jnp.int32)[None, :]
    select = (
        picked[:, :, None] == jnp.arange(history.shape[1], dtype=jnp.int32)[None, None, :]
    ).astype(jnp.float32)
    return jnp.einsum("skl,slc->skc", select, history.astype(jnp.float32), precision=HIGH).astype(
        jnp.bfloat16
    )


def replay_state(
    state, history_x, history_b, path_dt, conv_wx, conv_wb, accepted, rate_bias, a_rate, per_group
):
    seq_count, heads, head_dim, state_dim = state.shape
    path_len = path_dt.shape[1]
    path_xs = conv_window(history_x, conv_wx, path_len).reshape(
        seq_count, path_len, heads, head_dim
    )
    path_bs = conv_window(history_b, conv_wb, path_len).reshape(
        seq_count, path_len, heads // per_group, state_dim
    )
    path_bh = jnp.repeat(path_bs, per_group, axis=2)
    path_step = jax.nn.softplus(path_dt.astype(jnp.float32) + rate_bias)
    is_live = (jnp.arange(path_len, dtype=jnp.int32)[None, :] < accepted[:, None]).astype(
        jnp.float32
    )[:, :, None]
    log_decay = path_step * a_rate * is_live
    overall = jnp.sum(log_decay, axis=1)
    tail_sum = overall[:, None, :] - jnp.cumsum(log_decay, axis=1)
    weights = is_live * jnp.exp(tail_sum) * path_step
    grown = jnp.einsum("sjh,sjhp,sjhn->shpn", weights, path_xs, path_bh, precision=HIGH)
    return jnp.exp(overall)[:, :, None, None] * state + grown


def tree_links(parents, keep):
    seq_count, prop_count = parents.shape
    front = jnp.broadcast_to(jnp.arange(-1, keep - 1, dtype=jnp.int32)[None, :], (seq_count, keep))
    parent_ids = jnp.concatenate([front, parents + keep], axis=1)
    nodes = keep + prop_count
    links = (parent_ids[:, :, None] == jnp.arange(nodes, dtype=jnp.int32)[None, None, :]).astype(
        jnp.float32
    )
    identity = jnp.eye(prop_count, dtype=jnp.float32)[None, :, :]
    ancestry = identity + links[:, keep:, keep:]
    for turn in range(prop_count.bit_length()):
        ancestry = jnp.minimum(jnp.einsum("sij,sjk->sik", ancestry, ancestry, precision=HIGH), 1.0)
    return (links, ancestry)


def tree_conv(buffer, rows, taps, links, keep):
    values = jnp.concatenate([buffer, rows], axis=1).astype(jnp.float32)
    weights = taps.astype(jnp.float32)
    last_tap = weights.shape[0] - 1
    summed = weights[last_tap] * values
    reached = values
    for distance in range(1, last_tap + 1):
        reached = jnp.einsum("sij,sjc->sic", links, reached, precision=HIGH)
        summed = summed + weights[last_tap - distance] * reached
    return jax.nn.silu(summed[:, keep:, :])


def tree_mix(
    state,
    post_x,
    post_b,
    post_c,
    rate_rows,
    z_rows,
    ancestry,
    rate_bias,
    a_rate,
    d_skip,
    gain_out,
    per_group,
):
    seq_count, prop_count, _ = post_x.shape
    heads, head_dim, state_dim = (state.shape[1], state.shape[2], state.shape[3])
    groups = heads // per_group
    x_heads = post_x.reshape(seq_count, prop_count, heads, head_dim)
    b_groups = post_b.reshape(seq_count, prop_count, groups, state_dim)
    c_groups = post_c.reshape(seq_count, prop_count, groups, state_dim)
    step_size = jax.nn.softplus(rate_rows.astype(jnp.float32) + rate_bias)
    path_decay = jnp.einsum("sij,sjh->sih", ancestry, step_size * a_rate, precision=HIGH)
    c_heads = jnp.repeat(c_groups, per_group, axis=2)
    carried = (
        jnp.einsum("sihn,shpn->sihp", c_heads, state, precision=HIGH)
        * jnp.exp(path_decay)[:, :, :, None]
    )
    scores = jnp.einsum("sign,sjgn->sgij", c_groups, b_groups, precision=HIGH)
    scores = jnp.repeat(scores, per_group, axis=1)
    decay_t = jnp.transpose(path_decay, (0, 2, 1))
    decay_gap = decay_t[:, :, :, None] - decay_t[:, :, None, :]
    is_live = ancestry[:, None, :, :] > 0.5
    mixing = jnp.where(is_live, jnp.exp(jnp.where(is_live, decay_gap, 0.0)), 0.0)
    mixing = mixing * jnp.transpose(step_size, (0, 2, 1))[:, :, None, :]
    within = jnp.einsum("shij,sjhp->sihp", scores * mixing, x_heads, precision=HIGH)
    heads_out = carried + within + d_skip[None, None, :, None] * x_heads
    heads_out = heads_out.reshape(seq_count, prop_count, heads * head_dim) * jax.nn.silu(
        z_rows.astype(jnp.float32)
    )
    grouped = heads_out.reshape(seq_count, prop_count, groups, per_group * head_dim)
    grouped = grouped * lax.rsqrt(jnp.mean(grouped * grouped, axis=-1, keepdims=True) + EPS)
    return (grouped.reshape(seq_count, prop_count, heads * head_dim) * gain_out).astype(
        jnp.bfloat16
    )


def shards(
    tokens,
    parents,
    accepted,
    state,
    conv_x,
    conv_b,
    conv_c,
    path_x,
    path_b,
    path_c,
    path_dt,
    gain_in,
    w_x,
    w_z,
    w_b,
    w_c,
    w_dt,
    dt_bias,
    a_log,
    d_skip,
    conv_wx,
    conv_wb,
    conv_wc,
    gain_out,
    w_out,
):
    seq_local = state.shape[0]
    proposals = parents.shape[1]
    heads_local = dt_bias.shape[0]
    inner_local = w_x.shape[1]
    group_cols = w_b.shape[1]
    width = gain_in.shape[0]
    keep = conv_wx.shape[0] - 1
    tp_index = lax.axis_index("tp")
    whole_rows = exchange_by_axis(tokens, KV, (0, 1), 0, 2)
    flat_rows = whole_rows.reshape(-1, width).astype(jnp.float32)
    scaled = (flat_rows * gain_in).astype(jnp.bfloat16)
    joined = jnp.dot(
        scaled,
        jnp.concatenate(sent_together((w_x, w_z, w_b, w_c), KV, 0, 1), axis=1),
        preferred_element_type=jnp.float32,
    )
    w_rate = lax.dynamic_slice_in_dim(w_dt, tp_index * heads_local, heads_local, 1)
    rate_raw = jnp.dot(scaled, w_rate, preferred_element_type=jnp.float32)
    squares = jnp.sum(flat_rows * flat_rows, axis=1)
    row_scale = lax.rsqrt(squares / width + EPS)[:, None]

    def column_part(lower, upper):
        return (
            (joined[:, lower:upper] * row_scale)
            .astype(jnp.bfloat16)
            .reshape(seq_local, proposals, upper - lower)
        )

    x_rows = column_part(0, inner_local)
    z_rows = column_part(inner_local, 2 * inner_local)
    b_rows = column_part(2 * inner_local, 2 * inner_local + group_cols)
    c_rows = column_part(2 * inner_local + group_cols, 2 * inner_local + 2 * group_cols)
    rate_rows = (
        (rate_raw * row_scale).astype(jnp.bfloat16).reshape(seq_local, proposals, heads_local)
    )
    a_rate = -jnp.exp(a_log)
    history_x = jnp.concatenate([conv_x, path_x], axis=1)
    history_b = jnp.concatenate([conv_b, path_b], axis=1)
    history_c = jnp.concatenate([conv_c, path_c], axis=1)
    new_state = replay_state(
        state, history_x, history_b, path_dt, conv_wx, conv_wb, accepted, dt_bias, a_rate, HPG
    )
    links, ancestry = tree_links(parents, keep)
    post_x = tree_conv(commit_rows(history_x, accepted, keep), x_rows, conv_wx, links, keep)
    post_b = tree_conv(commit_rows(history_b, accepted, keep), b_rows, conv_wb, links, keep)
    post_c = tree_conv(commit_rows(history_c, accepted, keep), c_rows, conv_wc, links, keep)
    gated = tree_mix(
        new_state,
        post_x,
        post_b,
        post_c,
        rate_rows,
        z_rows,
        ancestry,
        dt_bias,
        a_rate,
        d_skip,
        gain_out,
        HPG,
    )
    gated_flat = gated.reshape(-1, inner_local)
    partial_out = jnp.dot(gated_flat, whole_of(w_out, KV, 1), preferred_element_type=jnp.float32)
    summed = sum_at_owner(partial_out.astype(jnp.bfloat16), "tp", 1)
    mixed = summed.astype(jnp.bfloat16).reshape(seq_local, proposals, -1)
    return (mixed, new_state)


def solution(mesh):
    finer = Mesh(mesh.devices.reshape(8, 4, mesh.shape["tp"]), ("kv_0", "kv_1", "tp"))
    return jax.shard_map(
        shards,
        mesh=finer,
        in_specs=(
            P(None, None, KV),
            P(KV, None),
            P(KV),
            P(KV, "tp", None, None),
            P(KV, None, "tp"),
            P(KV, None, "tp"),
            P(KV, None, "tp"),
            P(KV, None, "tp"),
            P(KV, None, "tp"),
            P(KV, None, "tp"),
            P(KV, None, "tp"),
            P(),
            P(KV, "tp"),
            P(KV, "tp"),
            P(KV, "tp"),
            P(KV, "tp"),
            P(),
            P("tp"),
            P("tp"),
            P("tp"),
            P(None, "tp"),
            P(None, "tp"),
            P(None, "tp"),
            P("tp"),
            P("tp", KV),
        ),
        out_specs=(P(KV, None, "tp"), P(KV, "tp", None, None)),
        check_vma=False,
    )
```

profile of v0, /device:TPU:1, one launch (start us, length us, event | category | flops | bytes accessed | tf_op | source)
XLA Modules:
  0.0 220.9 jit_solution(7903620484369633497)
XLA Ops:
  7.2 1.9 pad_maximum_fusion
  9.2 2.1 copy.139
  11.3 9.1 %all-to-all-start = ((bf16[8,4,8,12,128]{4,2,1,3,0:T(8,128)(2,1)}), bf16[8,4,8,12,128]{4,2,1,3,0:T(8,128)(2,1)S(1)}, u32[]{:S(2)}, u32[]{:S(2)}) async-start(bf16[8,4,8,12,128]{4,2,1,3,0:T(8,128)(2,1)} %copy.139), calls=%async_computation | async-start | bytes 1572864 | tf_op jit(solution)/shard_map/all_to_all | solution.py:31
  20.6 15.7 %all_gather.10 = bf16[512,512]{1,0:T(8,128)(2,1)} all-gather(bf16[512,128]{1,0:T(8,128)(2,1)S(1)} %copy-done.7), channel_id=1, replica_groups=mesh['kv_0'=8,'kv_1'=4,'tp'=8] {'kv_1'}, dimensions={1}, use_global_device_ids=true | all-gather | bytes 655360 | tf_op jit(solution)/shard_map/all_gather | solution.py:51
  40.5 0.8 broadcast_compare_fusion
  41.3 1.9 broadcast_multiply_fusion
  43.2 6.2 %all-to-all-done = bf16[8,4,8,12,128]{4,2,1,3,0:T(8,128)(2,1)S(1)} async-done(((bf16[8,4,8,12,128]{4,2,1,3,0:T(8,128)(2,1)}), bf16[8,4,8,12,128]{4,2,1,3,0:T(8,128)(2,1)S(1)}, u32[]{:S(2)}, u32[]{:S(2)}) %all-to-all-start) | async-done | bytes 786464 | tf_op jit(solution)/shard_map/all_to_all | solution.py:31
  49.3 1.1 copy.140
  50.4 4.0 %all-to-all-start.1 = ((bf16[8,4,8,12,128]{4,2,0,3,1:T(8,128)(2,1)}), bf16[8,4,8,12,128]{4,2,0,3,1:T(8,128)(2,1)S(1)}, u32[]{:S(2)}, u32[]{:S(2)}) async-start(bf16[8,4,8,12,128]{4,2,0,3,1:T(8,128)(2,1)} %copy.140), calls=%async_computation.1 | async-start | bytes 1572864 | tf_op jit(solution)/shard_map/all_to_all | solution.py:31
  54.5 1.0 fusion.53
  56.8 5.9 %multiply_add_fusion = f32[8,8,64,128]{3,2,1,0:T(8,128)} fusion(f32[8,8,64,128]{3,2,1,0:T(8,128)S(1)} %copy-done.2, f32[8,6,8,128]{3,1,2,0:T(8,128)S(1)} %bitcast.92, f32[8,8]{1,0:T(8,128)S(1)} %exp.57, f32[8,6,8,64]{3,2,0,1:T(8,128)} %broadcast_multiply_fusion), kind=kOutput, calls=%fused_computation.1 | convolution fusion | flops 38797312 | bytes 4489472 | tf_op jit(solution)/shard_map/sjh,sjhp,sjhn->shpn/dot_general | solution.py:100
  62.7 3.0 %all-to-all-done.1 = bf16[8,4,8,12,128]{4,2,0,3,1:T(8,128)(2,1)S(1)} async-done(((bf16[8,4,8,12,128]{4,2,0,3,1:T(8,128)(2,1)}), bf16[8,4,8,12,128]{4,2,0,3,1:T(8,128)(2,1)S(1)}, u32[]{:S(2)}, u32[]{:S(2)}) %all-to-all-start.1) | async-done | bytes 786464 | tf_op jit(solution)/shard_map/all_to_all | solution.py:31
  66.0 0.9 copy.142
  67.3 0.9 fusion.4
  70.1 68.7 %all-gather.3.cloned.1.call-done = bf16[4096,1536]{1,0:T(8,128)(2,1)} async-done(((bf16[128,1536]{1,0:T(8,128)(2,1)}), bf16[4096,1536]{1,0:T(8,128)(2,1)}) %all-gather.3.cloned.1.call-update) | async-done | bytes 12582928 | tf_op jit(solution)/shard_map/all_gather | solution.py:46
  138.8 7.3 %fusion.22 = f32[96,1536]{1,0:T(8,128)S(1)} fusion(bf16[4096,1536]{1,0:T(8,128)(2,1)} %all-gather.3.cloned.1.call-done, f32[12,8,32,128]{3,2,1,0:T(8,128)S(1)} %bitcast.86, f32[4096]{0:T(1024)S(1)} %copy-done.10), kind=kOutput, calls=%fused_computation.38 | convolution fusion | flops 1208745984 | bytes 14761984 | tf_op jit(solution)/shard_map/dot_general | solution.py:215
  148.1 1.0 multiply_bitcast_fusion
  151.6 0.9 reshape.190
  152.4 1.3 fusion.32
  154.0 1.7 fusion.6
  155.8 3.4 %fusion.113 = f32[8,8,64,12]{2,3,1,0:T(8,128)S(1)} fusion(f32[8,8,64,128]{3,2,1,0:T(8,128)S(1)} %copy-done.1, f32[8,12,8,128]{3,1,2,0:T(8,128)S(1)} %bitcast.91), kind=kOutput, calls=%fused_computation.187 | convolution fusion | flops 75497472 | bytes 2686976 | tf_op jit(solution)/shard_map/sihn,shpn->sihp/dot_general | solution.py:155
  160.4 32.7 %all-gather.5.cloned.1.call-done = bf16[512,4096]{1,0:T(8,128)(2,1)} async-done(((bf16[512,512]{1,0:T(8,128)(2,1)}), bf16[512,4096]{1,0:T(8,128)(2,1)}) %all-gather.5.cloned.1.call-update) | async-done | bytes 4194320 | tf_op jit(solution)/shard_map/all_gather | solution.py:51
  193.1 3.0 %convolution_convert_fusion = bf16[96,4096]{1,0:T(8,128)(2,1)S(1)} fusion(bf16[512,4096]{1,0:T(8,128)(2,1)} %all-gather.5.cloned.1.call-done, f32[96,512]{1,0:T(8,128)S(1)} %bitcast.93, f32[96,512]{1,0:T(8,128)S(1)} %reshape.185, f32[96,512]{1,0:T(8,128)S(1)} %get-tuple-element.15, f32[512]{0:T(512)S(1)} %copy-done.46), kind=kOutput, calls=%fused_computation | convolution fusion | flops 403439616 | bytes 5572608 | tf_op jit(solution)/shard_map/dot_general | solution.py:265
  196.2 17.1 %all_to_all.15 = bf16[8,96,512]{2,1,0:T(8,128)(2,1)S(1)} all-to-all(bf16[8,96,512]{2,1,0:T(8,128)(2,1)S(1)} %bitcast.89), channel_id=1, replica_groups=mesh['kv_0'=8,'kv_1'=4,'tp'=8] {'tp'}, dimensions={0} | all-to-all | bytes 1572864 | tf_op jit(solution)/shard_map/all_to_all | solution.py:57
  (197 shorter events, 14.1 us)
Async XLA Ops:
  7.2 60.1 %copy-start = (bf16[4096,64]{0,1:T(8,128)(2,1)S(1)}, bf16[4096,64]{0,1:T(8,128)(2,1)}, u32[]{:S(2)}) copy-start(bf16[4096,64]{0,1:T(8,128)(2,1)} %param.41) | copy-start | bytes 1572868
  7.2 13.4 %copy-start.7 = (bf16[512,128]{1,0:T(8,128)(2,1)S(1)}, bf16[512,128]{1,0:T(8,128)(2,1)}, u32[]{:S(2)}) copy-start(bf16[512,128]{1,0:T(8,128)(2,1)} %param.49) | copy-start | bytes 393220
  7.2 131.6 %all-gather.3.cloned.1.call-start = ((), (), s32[]{:S(2)}) async-start(), calls=%async_computation.3 | async-start | bytes 12976128 | tf_op jit(solution)/shard_map/all_gather | solution.py:46
  9.1 27.2 %copy-start.47 = (s32[8]{0:T(128)S(1)}, s32[8]{0:T(128)}, u32[]{:S(2)}) copy-start(s32[8]{0:T(128)} %param.27) | copy-start | bytes 100
  9.1 27.2 %copy-start.13 = (bf16[8,6,256]{2,0,1:T(8,128)(2,1)S(1)}, bf16[8,6,256]{2,0,1:T(8,128)(2,1)}, u32[]{:S(2)}) copy-start(bf16[8,6,256]{2,0,1:T(8,128)(2,1)} %param.33) | copy-start | bytes 73732
  9.2 27.2 %copy-start.26 = (bf16[8,3,256]{2,0,1:T(8,128)(2,1)S(1)}, bf16[8,3,256]{2,0,1:T(8,128)(2,1)}, u32[]{:S(2)}) copy-start(bf16[8,3,256]{2,0,1:T(8,128)(2,1)} %param.30) | copy-start | bytes 36868
  9.2 27.5 %copy-start.12 = (bf16[8,6,512]{2,0,1:T(8,128)(2,1)S(1)}, bf16[8,6,512]{2,0,1:T(8,128)(2,1)}, u32[]{:S(2)}) copy-start(bf16[8,6,512]{2,0,1:T(8,128)(2,1)} %param.32) | copy-start | bytes 147460
  9.2 27.5 %copy-start.14 = (bf16[8,3,512]{2,0,1:T(8,128)(2,1)S(1)}, bf16[8,3,512]{2,0,1:T(8,128)(2,1)}, u32[]{:S(2)}) copy-start(bf16[8,3,512]{2,0,1:T(8,128)(2,1)} %param.29) | copy-start | bytes 73732
  11.3 25.7 %copy-start.41 = (s32[8,12]{1,0:T(8,128)S(1)}, s32[8,12]{1,0:T(8,128)}, u32[]{:S(2)}) copy-start(s32[8,12]{1,0:T(8,128)} %param.26) | copy-start | bytes 1156
  11.3 25.7 %copy-start.15 = (bf16[8,6,256]{2,0,1:T(8,128)(2,1)S(1)}, bf16[8,6,256]{2,0,1:T(8,128)(2,1)}, u32[]{:S(2)}) copy-start(bf16[8,6,256]{2,0,1:T(8,128)(2,1)} %param.34) | copy-start | bytes 73732
  11.3 26.3 %copy-start.27 = (bf16[8,3,256]{2,0,1:T(8,128)(2,1)S(1)}, bf16[8,3,256]{2,0,1:T(8,128)(2,1)}, u32[]{:S(2)}) copy-start(bf16[8,3,256]{2,0,1:T(8,128)(2,1)} %param.31) | copy-start | bytes 36868
  11.3 26.3 %copy-start.36 = (bf16[4,256]{1,0:T(4,128)(2,1)S(1)}, bf16[4,256]{1,0:T(4,128)(2,1)}, u32[]{:S(2)}) copy-start(bf16[4,256]{1,0:T(4,128)(2,1)} %param.46) | copy-start | bytes 6148
  11.3 26.4 %copy-start.24 = (bf16[4,512]{1,0:T(4,128)(2,1)S(1)}, bf16[4,512]{1,0:T(4,128)(2,1)}, u32[]{:S(2)}) copy-start(bf16[4,512]{1,0:T(4,128)(2,1)} %param.45) | copy-start | bytes 12292
  11.3 38.0 %all-to-all-start = ((bf16[8,4,8,12,128]{4,2,1,3,0:T(8,128)(2,1)}), bf16[8,4,8,12,128]{4,2,1,3,0:T(8,128)(2,1)S(1)}, u32[]{:S(2)}, u32[]{:S(2)}) async-start(bf16[8,4,8,12,128]{4,2,1,3,0:T(8,128)(2,1)} %copy.139), calls=%async_computation | async-start | bytes 1572864 | tf_op jit(solution)/shard_map/all_to_all | solution.py:31
  20.5 18.8 %copy-start.49 = (f32[8]{0:T(128)S(1)}, f32[8]{0:T(128)}, u32[]{:S(2)}) copy-start(f32[8]{0:T(128)} %param.43) | copy-start | bytes 100
  20.5 18.8 %copy-start.9 = (bf16[8,6,8]{2,0,1:T(8,128)(2,1)S(1)}, bf16[8,6,8]{2,0,1:T(8,128)(2,1)}, u32[]{:S(2)}) copy-start(bf16[8,6,8]{2,0,1:T(8,128)(2,1)} %param.35) | copy-start | bytes 2308
  20.5 18.8 %copy-start.25 = (f32[8]{0:T(128)S(1)}, f32[8]{0:T(128)}, u32[]{:S(2)}) copy-start(f32[8]{0:T(128)} %param.42) | copy-start | bytes 100
  20.5 172.6 %all-gather.5.cloned.1.call-start = ((), (), s32[]{:S(2)}) async-start(), calls=%async_computation.4 | async-start | bytes 4718592 | tf_op jit(solution)/shard_map/all_gather | solution.py:51
  40.2 15.2 %copy-start.37 = (bf16[4,256]{1,0:T(4,128)(2,1)S(1)}, bf16[4,256]{1,0:T(4,128)(2,1)}, u32[]{:S(2)}) copy-start(bf16[4,256]{1,0:T(4,128)(2,1)} %param.47) | copy-start | bytes 6148
  41.3 15.5 %copy-start.2 = (f32[8,8,64,128]{3,2,1,0:T(8,128)S(1)}, f32[8,8,64,128]{3,2,1,0:T(8,128)}, u32[]{:S(2)}) copy-start(f32[8,8,64,128]{3,2,1,0:T(8,128)} %param.28) | copy-start | bytes 6291460
  50.4 15.3 %all-to-all-start.1 = ((bf16[8,4,8,12,128]{4,2,0,3,1:T(8,128)(2,1)}), bf16[8,4,8,12,128]{4,2,0,3,1:T(8,128)(2,1)S(1)}, u32[]{:S(2)}, u32[]{:S(2)}) async-start(bf16[8,4,8,12,128]{4,2,0,3,1:T(8,128)(2,1)} %copy.140), calls=%async_computation.1 | async-start | bytes 1572864 | tf_op jit(solution)/shard_map/all_to_all | solution.py:31
  151.6 4.2 %copy-start.4 = (f32[8,12,2,128]{3,1,2,0:T(8,128)S(1)}, f32[8,12,2,128]{3,1,2,0:T(8,128)}, u32[]{:S(2)}) copy-start(f32[8,12,2,128]{3,1,2,0:T(8,128)} %copy.150) | copy-start | bytes 294916
  151.6 4.3 %copy-start.1 = (f32[8,8,64,128]{3,2,1,0:T(8,128)S(1)}, f32[8,8,64,128]{3,2,1,0:T(8,128)}, u32[]{:S(2)}) copy-start(f32[8,8,64,128]{3,2,1,0:T(8,128)} %multiply_add_fusion) | copy-start | bytes 6291460
  159.2 33.9 %copy-start.46 = (f32[512]{0:T(512)S(1)}, f32[512]{0:T(512)}, u32[]{:S(2)}) copy-start(f32[512]{0:T(512)} %param.48) | copy-start | bytes 6148
  (30 other events, 56.6 us)
Sparse Core Ops, SparseCore 0:
  10.6 128.1 all-gather.2
  140.6 52.4 all-gather.4
where the time goes:
time: 222 us; the launch traced here: 221 us
  waiting for transfers between devices  111 us (50%)
  blocking collectives  32.7 us (15%)
  matrix products  28.9 us (13%)
  between operations  15.2 us (7%)
  starting transfers between devices  13.2 us (6%)
  local copies, waits for them, and re-layouts  12.4 us (6%)
  other arithmetic  7.79 us (4%)
    all_gather x1, waiting for transfers between devices, sent_together(): lax.all_gather(both, axis, axis=dim, tiled=True)  68.7 us
    all_gather x1, waiting for transfers between devices, whole_of(): x = lax.all_gather(x, axis, axis=dim, tiled=True)  32.7 us
    all_to_all x1, blocking collectives, sum_at_owner(): lax.all_to_all(blocks, axis, split_axis=0, concat_axis=0, tiled=True)  17.1 us
    all_gather x1, blocking collectives, whole_of(): x = lax.all_gather(x, axis, axis=dim, tiled=True)  15.7 us
    all_to_all x2, starting transfers between devices, turned_blocks(): out = lax.all_to_all(out, axes[k], k, k, tiled=True)  13.2 us
    all_to_all x2, waiting for transfers between devices, turned_blocks(): out = lax.all_to_all(out, axes[k], k, k, tiled=True)  9.24 us
    dot_general x1, matrix products, shards(): jnp.dot(scaled, jnp.concatenate(sent_together((w_x, w_z, w_b, w_c), KV, 0...  7.29 us
    dot_general x1, matrix products, replay_state(): jnp.einsum('sjh,sjhp,sjhn->shpn', weights, path_xs, path_bh, precision=HIGH)  5.93 us
  transfers between devices with their start and end apart: 4, of which 4 were waited for; matrix products, arithmetic and copies ran while one was open for 19% of the time, Pallas kernels for 0%

commit v1 on v0

v1 whole, which is shorter than its diff:
```python
import functools

import jax
import jax.numpy as jnp
from jax import lax
from jax.experimental import pallas as pl
from jax.experimental.pallas import tpu as pltpu
from jax.sharding import Mesh
from jax.sharding import PartitionSpec as P

NZ, NX, NY, NC = 8, 4, 4, 2
NT = NY * NC
MESH = pl.DeviceIdType.MESH
KV = ("z", "x")
TP = ("y", "c")
EPS = 1e-06
HIGH = lax.Precision.HIGHEST
F32 = jnp.float32
BF16 = jnp.bfloat16
NQ, NS, NP, NH = 12, 8, 6, 8
VMEM_LIMIT = 60 * 1024 * 1024


def wrap(i, n):
    return lax.rem(i + n, n)


def remote(src, dst, send_sem, recv_sem, device):
    return pltpu.make_async_remote_copy(
        src_ref=src,
        dst_ref=dst,
        send_sem=send_sem,
        recv_sem=recv_sem,
        device_id=device,
        device_id_type=MESH,
    )


def greet(devices):
    barrier = pltpu.get_barrier_semaphore()
    for device in devices:
        pl.semaphore_signal(barrier, inc=1, device_id=device, device_id_type=MESH)
    pl.semaphore_wait(barrier, len(devices))


def hops_of(piece, way):
    return 4 if (piece % 2 == 0) == (way == 0) else 3


def inproj_kernel(
    tok,
    wx,
    wz,
    wb,
    wc,
    wr,
    gain,
    wo,
    rows_out,
    aux_out,
    wog,
    tg,
    ts,
    wg,
    prod,
    aprod,
    ring,
    aring,
    stage,
    astage,
    t_s,
    t_r,
    f_s,
    f_r,
    w_s,
    w_r,
    r_s,
    r_r,
    o_s,
    o_r,
):
    z, x, c = lax.axis_index("z"), lax.axis_index("x"), lax.axis_index("c")
    greet(
        [{"x": wrap(x + d, NX)} for d in (1, 2, 3)]
        + [{"z": wrap(z + 1, NZ)}, {"z": wrap(z - 1, NZ)}, {"c": 1 - c}]
    )
    half = pl.ds(4 * c, 4)

    def tok_copy(d):
        to = wrap(x + d, NX)
        return remote(
            tok.at[:, half, to], tg.at[x, :, half], t_s.at[d - 1], t_r.at[d - 1], {"x": to}
        )

    def tok_share(d):
        block = tg.at[wrap(x - d, NX), :, half]
        return remote(block, block, f_s.at[d - 1], f_r.at[d - 1], {"c": 1 - c})

    pieces = [
        wx.at[:, 0:256],
        wx.at[:, 256:512],
        wz.at[:, 0:256],
        wz.at[:, 256:512],
        wb,
        wc,
    ]

    def depth_of(owner):
        return pl.ds(pl.multiple_of(owner * 128, 128), 128)

    def w_own(p, way):
        to = wrap(x + (1 if way == 0 else -1), NX)
        return remote(
            pieces[p], wg.at[p, depth_of(x), :], w_s.at[p, way], w_r.at[p, way], {"x": to}
        )

    def w_pass(p):
        sign = 1 if p % 2 == 0 else -1
        block = wg.at[p, depth_of(wrap(x - sign, NX)), :]
        return remote(block, block, w_s.at[p, 2], w_r.at[p, 2], {"x": wrap(x + sign, NX)})

    def o_copy(way, hop):
        sign = 1 if way == 0 else -1
        owner = wrap(z - sign * (hop - 1), NZ)
        src = wo if hop == 1 else wog.at[owner]
        dst = wog.at[owner]
        if hop == 4:
            src, dst = src.at[pl.ds(256 * way, 256)], dst.at[pl.ds(256 * way, 256)]
        return remote(
            src, dst, o_s.at[way, hop - 1], o_r.at[way, hop - 1], {"z": wrap(z + sign, NZ)}
        )

    def r_copy(p, way, hop):
        sign = 1 if way == 0 else -1
        to = {"z": wrap(z + sign, NZ)}
        if p == 6:
            src = astage.at[way] if hop == 1 else aring.at[way, hop - 2]
            dst = aring.at[way, hop - 1]
        else:
            src = stage.at[p, way] if hop == 1 else ring.at[p, way, hop - 2]
            dst = ring.at[p, way, hop - 1]
        return remote(src, dst, r_s.at[p, way, hop - 1], r_r.at[p, way, hop - 1], to)

    def own_term(p, dest):
        if p == 6:
            return aprod[:, pl.ds(dest, 1)].reshape(NQ, NS, 128)
        return prod[p, :, pl.ds(dest, 1)].reshape(NQ, NS, 256)

    def r_step(p, hop):
        for way in (0, 1):
            hops = hops_of(p, way)
            if hop > hops:
                continue
            sign = 1 if way == 0 else -1
            term = own_term(p, wrap(z + sign * (hops + 1 - hop), NZ))
            if hop == 1:
                if p == 6:
                    astage[way] = term.astype(BF16)
                else:
                    stage[p, way] = term.astype(BF16)
            else:
                r_copy(p, way, hop - 1).wait_recv()
                if p == 6:
                    aring[way, hop - 2] = (aring[way, hop - 2].astype(F32) + term).astype(BF16)
                else:
                    ring[p, way, hop - 2] = (ring[p, way, hop - 2].astype(F32) + term).astype(BF16)
            r_copy(p, way, hop).start()

    def r_total(p):
        total = own_term(p, z)
        for way in (0, 1):
            hops = hops_of(p, way)
            r_copy(p, way, hops).wait_recv()
            arrived = aring[way, hops - 1] if p == 6 else ring[p, way, hops - 1]
            total = total + arrived.astype(F32)
        return total.reshape(NQ * NS, total.shape[2])

    order = (1, 3, 2)
    for d in order:
        tok_copy(d).start()
    for p in range(6):
        first = p % 2
        w_own(p, first).start()
        w_own(p, 1 - first).start()
    for way in (0, 1):
        o_copy(way, 1).start()
    tg[pl.ds(x, 1)] = tok[:, :, pl.ds(x, 1)].reshape(1, NQ, NZ, NS, 128)
    for p in range(6):
        wg[p, depth_of(x), :] = pieces[p][...]
    wog[pl.ds(z, 1)] = wo[...].reshape(1, 512, 128)
    for d in order:
        tok_copy(d).wait_recv()
        tok_share(d).start()
    for way in (0, 1):
        o_copy(way, 1).wait_recv()
        o_copy(way, 2).start()
    for d in order:
        tok_share(d).wait_recv()

    squares = jnp.zeros((NQ * NZ * NS, 128), F32)
    for xs in range(NX):
        values = tg[xs].reshape(NQ * NZ * NS, 128).astype(F32)
        squares = squares + values * values
        ts[:, xs * 128 : (xs + 1) * 128] = (values * gain[pl.ds(z * NX + xs, 1), :]).astype(BF16)
    lane = lax.broadcasted_iota(jnp.int32, (NQ * NZ * NS, 128), 1)
    rates = lax.dot_general(
        ts[...], wr[...], (((1,), (1,)), ((), ())), preferred_element_type=F32
    )
    sums = jnp.sum(squares, axis=1, keepdims=True)
    aprod[...] = jnp.where(lane == 8, sums, rates).reshape(NQ, NZ, NS, 128)
    r_step(6, 1)

    def forward(ch):
        for p in (2 * ch, 2 * ch + 1):
            w_own(p, p % 2).wait_recv()
            w_pass(p).start()

    def multiply(ch):
        for p in (2 * ch, 2 * ch + 1):
            w_own(p, 1 - p % 2).wait_recv()
            w_pass(p).wait_recv()
            prod[p] = jnp.dot(ts[...], wg[p], preferred_element_type=F32).reshape(
                NQ, NZ, NS, 256
            )
            r_step(p, 1)

    def advance(ch, hop):
        for p in (2 * ch, 2 * ch + 1):
            r_step(p, hop)

    forward(0)
    forward(1)
    multiply(0)
    for way in (0, 1):
        o_copy(way, 2).wait_recv()
        o_copy(way, 3).start()
    r_step(6, 2)
    advance(0, 2)
    forward(2)
    multiply(1)
    for way in (0, 1):
        o_copy(way, 3).wait_recv()
        o_copy(way, 4).start()
    r_step(6, 3)
    advance(0, 3)
    advance(1, 2)
    multiply(2)
    r_step(6, 4)
    advance(0, 4)
    advance(1, 3)
    advance(2, 2)
    advance(1, 4)
    advance(2, 3)
    advance(2, 4)

    total = r_total(6)
    scale = lax.rsqrt(total[:, 8:9] / (NZ * NX * 128.0) + EPS)
    aux_out[...] = (total * scale).astype(BF16).astype(F32)
    for p in range(6):
        rows_out[:, p * 256 : (p + 1) * 256] = (r_total(p) * scale).astype(BF16)

    for way in (0, 1):
        o_copy(way, 4).wait_recv()
        for hop in (1, 2, 3, 4):
            o_copy(way, hop).wait_send()
    for d in order:
        tok_copy(d).wait_send()
        tok_share(d).wait_send()
    for p in range(6):
        w_own(p, 0).wait_send()
        w_own(p, 1).wait_send()
        w_pass(p).wait_send()
    for p in range(7):
        for way in (0, 1):
            for hop in range(1, hops_of(p, way) + 1):
                r_copy(p, way, hop).wait_send()


def inproj(tok, wx, wz, wb, wc, wr, gain, wo):
    vmem = pl.BlockSpec(memory_space=pltpu.VMEM)
    dma = pltpu.SemaphoreType.DMA
    return pl.pallas_call(
        inproj_kernel,
        name="inproj",
        out_shape=(
            jax.ShapeDtypeStruct((NQ * NS, 1536), BF16),
            jax.ShapeDtypeStruct((NQ * NS, 128), F32),
            jax.ShapeDtypeStruct((NZ, 512, 128), BF16),
        ),
        in_specs=[vmem] * 8,
        out_specs=(vmem, vmem, vmem),
        scratch_shapes=[
            pltpu.VMEM((NX, NQ, NZ, NS, 128), BF16),
            pltpu.VMEM((NQ * NZ * NS, 512), BF16),
            pltpu.VMEM((6, 512, 256), BF16),
            pltpu.VMEM((6, NQ, NZ, NS, 256), F32),
            pltpu.VMEM((NQ, NZ, NS, 128), F32),
            pltpu.VMEM((6, 2, 4, NQ, NS, 256), BF16),
            pltpu.VMEM((2, 4, NQ, NS, 128), BF16),
            pltpu.VMEM((6, 2, NQ, NS, 256), BF16),
            pltpu.VMEM((2, NQ, NS, 128), BF16),
            dma((3,)),
            dma((3,)),
            dma((3,)),
            dma((3,)),
            dma((6, 3)),
            dma((6, 3)),
            dma((7, 2, 4)),
            dma((7, 2, 4)),
            dma((2, 4)),
            dma((2, 4)),
        ],
        compiler_params=pltpu.CompilerParams(
            collective_id=0, has_side_effects=True, vmem_limit_bytes=VMEM_LIMIT
        ),
    )(tok, wx, wz, wb, wc, wr, gain, wo)


def silu(v):
    return v * (1.0 / (1.0 + jnp.exp(-v)))


def softplus(v):
    return jnp.maximum(v, 0.0) + jnp.log1p(jnp.exp(-jnp.abs(v)))


def mix_kernel(
    idx,
    rows,
    aux,
    cx,
    px,
    cb,
    pb,
    cc,
    pc,
    pdt,
    state,
    bias,
    alog,
    dskip,
    wtx,
    wtb,
    wtc,
    gain,
    gated,
    new_state,
):
    count = NQ * NS

    def iota(shape, dim):
        return lax.broadcasted_iota(jnp.int32, shape, dim)

    def dot(a, b):
        return jnp.dot(a.astype(BF16), b.astype(BF16), preferred_element_type=F32)

    def dot_of(a, b, dims, precision=None):
        return lax.dot_general(
            a, b, ((dims[:1], dims[1:]), ((), ())), precision=precision, preferred_element_type=F32
        )

    def past(first, last):
        return jnp.concatenate([first[...].astype(F32), last[...].astype(F32)], axis=0)

    spread = (iota((NH, 512), 1) // 64 == iota((NH, 512), 0)).astype(F32)

    def widen(v):
        return dot_of(v, spread, (1, 0), HIGH)

    rate = -jnp.exp(alog[...])
    hist_x, hist_b, hist_c = past(cx, px), past(cb, pb), past(cc, pc)
    tx, tb, tc = wtx[...].astype(F32), wtb[...].astype(F32), wtc[...].astype(F32)

    def window(history, taps):
        summed = taps[0:1] * history[0 : NP * NS]
        for k in (1, 2, 3):
            summed = summed + taps[k : k + 1] * history[k * NS : (k + NP) * NS]
        return silu(summed)

    path_xs, path_bs = window(hist_x, tx), window(hist_b, tb)
    path_step = softplus(pdt[...].astype(F32) + bias[...])
    live = (iota((NP * NS, 1), 0) // NS < idx[0 : NP * NS, 4:5]).astype(F32)
    path_log = path_step * rate * live
    tails = [jnp.zeros((NS, NH), F32)]
    for j in range(NP - 1, 0, -1):
        tails.insert(0, tails[0] + path_log[j * NS : (j + 1) * NS])
    overall = jnp.exp(tails[0] + path_log[0:NS])
    weights = live * jnp.exp(jnp.concatenate(tails, axis=0)) * path_step
    weighted = (path_xs * widen(weights)).astype(BF16)

    step = softplus(aux[:, 0:NH] + bias[...])
    slope = step * rate
    links = (iota((count, count), 1) == idx[:, 3:4]).astype(F32)
    eye = (iota((count, count), 0) == iota((count, count), 1)).astype(F32)
    family = eye + links
    for _ in range(4):
        family = jnp.minimum(dot(family, family), 1.0)
    is_kin = family > 0.5
    nodes = iota((count, 9 * NS + count), 1)
    one = (nodes == idx[:, 0:1]).astype(F32)
    two = dot(links, one) + (nodes == idx[:, 1:2]).astype(F32)
    three = dot(links, two) + (nodes == idx[:, 2:3]).astype(F32)
    one, two, three = one.astype(BF16), two.astype(BF16), three.astype(BF16)

    def tree_conv(history, own, taps):
        own = own.astype(F32)
        values = jnp.concatenate([history, own], axis=0).astype(BF16)
        summed = taps[3:4] * own
        for k, reach in ((2, one), (1, two), (0, three)):
            summed = summed + taps[k : k + 1] * dot(reach, values)
        return silu(summed)

    post_x = tree_conv(hist_x, rows[:, 0:512], tx)
    post_b = tree_conv(hist_b, rows[:, 1024:1280], tb).astype(BF16)
    post_c = tree_conv(hist_c, rows[:, 1280:1536], tc).astype(BF16)

    decay = dot_of(family, slope, (1, 0), HIGH)
    decay_t = dot_of(slope, family, (0, 1), HIGH)
    step_t = dot_of(step, eye, (0, 1), HIGH)
    grown = widen(jnp.exp(decay))
    skip = widen(jnp.broadcast_to(dskip[...], (NS, NH)))[0:1]
    post_xb = post_x.astype(BF16)
    seq_of = lax.rem(iota((count, 128), 0), NS)
    path_seq = lax.rem(iota((NP * NS, 128), 0), NS)
    lane = iota((count, 128), 1)

    for g in range(2):
        wide, narrow = slice(256 * g, 256 * g + 256), slice(128 * g, 128 * g + 128)
        post_bg, post_cg = post_b[:, narrow], post_c[:, narrow]
        split_b = jnp.concatenate(
            [jnp.where(path_seq == s, path_bs[:, narrow], 0.0) for s in range(NS)], axis=1
        ).astype(BF16)
        gained = dot_of(weighted[:, wide], split_b, (0, 0))
        carried = jnp.zeros((count, 256), F32)
        for s in range(NS):
            fade = jnp.concatenate(
                [
                    jnp.broadcast_to(overall[s : s + 1, h : h + 1], (64, 128))
                    for h in range(4 * g, 4 * g + 4)
                ],
                axis=0,
            )
            fresh = fade * state[s, wide, :] + gained[:, 128 * s : 128 * s + 128]
            new_state[s, wide, :] = fresh
            mine = jnp.where(seq_of == s, post_cg.astype(F32), 0.0).astype(BF16)
            carried = carried + dot_of(mine, fresh.astype(BF16), (1, 1))
        scores = dot_of(post_cg, post_bg, (1, 1))
        within = []
        for pair in range(2):
            sides = []
            for h in (4 * g + 2 * pair, 4 * g + 2 * pair + 1):
                gap = decay[:, h : h + 1] - decay_t[h : h + 1, :]
                mixing = jnp.exp(jnp.where(is_kin, gap, 0.0)) * step_t[h : h + 1, :]
                mixing = jnp.where(is_kin, scores * mixing, 0.0)
                at = 256 * g + 128 * pair
                sides.append(dot(mixing, post_xb[:, at : at + 128]))
            within.append(jnp.where(lane < 64, sides[0], sides[1]))
        heads = carried * grown[:, wide] + jnp.concatenate(within, axis=1)
        heads = heads + skip[:, wide] * post_x[:, wide]
        heads = heads * silu(rows[:, 512 + 256 * g : 768 + 256 * g].astype(F32))
        spread_of = jnp.sum(heads * heads, axis=1, keepdims=True) / 256.0
        heads = heads * lax.rsqrt(spread_of + EPS) * gain[:, wide]
        gated[:, wide] = heads.astype(BF16)


def mix(*args):
    vmem = pl.BlockSpec(memory_space=pltpu.VMEM)
    return pl.pallas_call(
        mix_kernel,
        name="mix",
        out_shape=(
            jax.ShapeDtypeStruct((NQ * NS, 512), BF16),
            jax.ShapeDtypeStruct((NS, 512, 128), F32),
        ),
        in_specs=[vmem] * len(args),
        out_specs=(vmem, vmem),
        compiler_params=pltpu.CompilerParams(vmem_limit_bytes=VMEM_LIMIT),
    )(*args)


def outproj_kernel(gated, wog, mixed, gg, woc, part, terms, g_s, g_r, p_s, p_r):
    x, y, c = lax.axis_index("x"), lax.axis_index("y"), lax.axis_index("c")
    t = y * NC + c

    def place(xs, tt):
        return {"x": xs, "y": tt // NC, "c": lax.rem(tt, NC)}

    greet(
        [
            place(wrap(x + d, NX), wrap(t + e, NT))
            for d in range(NX)
            for e in range(NT)
            if d + e > 0
        ]
    )

    def g_copy(d):
        return remote(
            gated, gg.at[d - 1], g_s.at[d - 1], g_r.at[d - 1], {"x": wrap(x + d, NX)}
        )

    def p_copy(d, e):
        tt = wrap(t + e, NT)
        return remote(
            part.at[d, tt],
            terms.at[x * NT + t],
            p_s.at[d, e],
            p_r.at[d, e],
            place(wrap(x - d, NX), tt),
        )

    order = (1, 3, 2)
    for d in order:
        g_copy(d).start()
    for k in range(NZ):
        woc[:, k * 128 : (k + 1) * 128] = wog[k]
    for d in (0,) + order:
        if d > 0:
            g_copy(d).wait_recv()
        values = gated[...] if d == 0 else gg[d - 1]
        for pair in range(4):
            cols = slice(256 * pair, 256 * pair + 256)
            product = jnp.dot(values, woc[:, cols], preferred_element_type=F32).astype(BF16)
            part[d, 2 * pair] = product[:, 0:128]
            part[d, 2 * pair + 1] = product[:, 128:256]
        for e in range(NT):
            if d + e > 0:
                p_copy(d, e).start()
    terms[pl.ds(x * NT + t, 1)] = part[0, pl.ds(t, 1)]
    for d in (0,) + order:
        for e in range(NT):
            if d + e > 0:
                p_copy(d, e).wait_recv()
    for xs in range(NX):
        total = terms[xs * NT].astype(F32)
        for k in range(1, NT):
            total = total + terms[xs * NT + k].astype(F32)
        mixed[:, xs * 128 : (xs + 1) * 128] = total.astype(BF16)
    for d in range(NX):
        if d > 0:
            g_copy(d).wait_send()
        for e in range(NT):
            if d + e > 0:
                p_copy(d, e).wait_send()


def outproj(gated, wog):
    vmem = pl.BlockSpec(memory_space=pltpu.VMEM)
    dma = pltpu.SemaphoreType.DMA
    return pl.pallas_call(
        outproj_kernel,
        name="outproj",
        out_shape=jax.ShapeDtypeStruct((NQ * NS, 512), BF16),
        in_specs=[vmem, vmem],
        out_specs=vmem,
        scratch_shapes=[
            pltpu.VMEM((3, NQ * NS, 512), BF16),
            pltpu.VMEM((512, 1024), BF16),
            pltpu.VMEM((NX, NT, NQ * NS, 128), BF16),
            pltpu.VMEM((NX * NT, NQ * NS, 128), BF16),
            dma((3,)),
            dma((3,)),
            dma((NX, NT)),
            dma((NX, NT)),
        ],
        compiler_params=pltpu.CompilerParams(
            collective_id=1, has_side_effects=True, vmem_limit_bytes=VMEM_LIMIT
        ),
    )(gated, wog)


def by_place(v):
    v = jnp.transpose(v, (1, 0, 2))
    return v.reshape(v.shape[0] * v.shape[1], v.shape[2])


def shards(
    tokens,
    parents,
    accepted,
    state,
    conv_x,
    conv_b,
    conv_c,
    path_x,
    path_b,
    path_c,
    path_dt,
    gain_in,
    w_x,
    w_z,
    w_b,
    w_c,
    w_dt,
    dt_bias,
    a_log,
    d_skip,
    conv_wx,
    conv_wb,
    conv_wc,
    gain_out,
    w_out,
):
    z = lax.axis_index("z")
    t = lax.axis_index("y") * NC + lax.axis_index("c")
    tok = jnp.transpose(tokens, (1, 0, 2)).reshape(NQ, NZ, NX, NS, 128)
    wr = lax.dynamic_slice(w_dt.T, (t * NH, z * 512), (NH, 512))
    wr = jnp.pad(wr, ((0, 128 - NH), (0, 0)))
    rows, aux, wog = inproj(tok, w_x, w_z, w_b, w_c, wr, gain_in.reshape(32, 128), w_out)

    up = parents.T
    seq = jnp.arange(NS, dtype=jnp.int32)[None, :]
    acc = accepted[None, :]
    root = up < 0
    idx = jnp.stack(
        [
            jnp.where(root, (acc + 2) * NS + seq, 9 * NS + up * NS + seq),
            jnp.where(root, (acc + 1) * NS + seq, -1),
            jnp.where(root, acc * NS + seq, -1),
            jnp.where(root, -1, up * NS + seq),
            jnp.broadcast_to(acc, up.shape),
        ],
        axis=-1,
    ).reshape(NQ * NS, 5)
    gated, new_state = mix(
        idx,
        rows,
        aux,
        by_place(conv_x),
        by_place(path_x),
        by_place(conv_b),
        by_place(path_b),
        by_place(conv_c),
        by_place(path_c),
        by_place(path_dt),
        state.reshape(NS, 512, 128),
        dt_bias[None, :],
        a_log[None, :],
        d_skip[None, :],
        conv_wx,
        conv_wb,
        conv_wc,
        gain_out[None, :],
    )
    mixed = outproj(gated, wog)
    mixed = jnp.transpose(mixed.reshape(NQ, NS, 512), (1, 0, 2))
    return (mixed, new_state.reshape(NS, NH, 64, 128))


def solution(mesh):
    finer = Mesh(mesh.devices.reshape(NZ, NX, NY, NC), ("z", "x", "y", "c"))
    return jax.shard_map(
        shards,
        mesh=finer,
        in_specs=(
            P(None, None, KV),
            P(KV, None),
            P(KV),
            P(KV, TP, None, None),
            P(KV, None, TP),
            P(KV, None, TP),
            P(KV, None, TP),
            P(KV, None, TP),
            P(KV, None, TP),
            P(KV, None, TP),
            P(KV, None, TP),
            P(),
            P(KV, TP),
            P(KV, TP),
            P(KV, TP),
            P(KV, TP),
            P(),
            P(TP),
            P(TP),
            P(TP),
            P(None, TP),
            P(None, TP),
            P(None, TP),
            P(TP),
            P(TP, KV),
        ),
        out_specs=(P(KV, None, TP), P(KV, TP, None, None)),
        check_vma=False,
    )
```

time: 222 us -> 96.1 us (0.43)
  waiting for transfers between devices: 111 us -> 0 us
  Pallas kernels: 0 us -> 89 us
  blocking collectives: 32.7 us -> 0 us
  matrix products: 28.9 us -> 0 us
  between operations: 15.2 us -> 0.69 us
  starting transfers between devices: 13.2 us -> 0 us
  local copies, waits for them, and re-layouts: 12.4 us -> 4.69 us
  other arithmetic: 7.79 us -> 1.48 us
    all_gather x2 -> x0, waiting for transfers between devices: 101 us -> none  [the longest x1 68.7 us: sent_together(): lax.all_gather(both, axis, axis=dim, tiled=True)]
    pallas_call x0 -> x3, Pallas kernels: none -> 89 us  [the longest x1 56.7 us: inproj(): pl.pallas_call(inproj_kernel, name='inproj', out_shape=(jax.ShapeDtypeStr...]
    dot_general x24 -> x0, matrix products: 28.9 us -> none  [the longest x1 7.29 us: shards(): jnp.dot(scaled, jnp.concatenate(sent_together((w_x, w_z, w_b, w_c), KV, 0...]
    all_to_all x1 -> x0, blocking collectives: 17.1 us -> none  [sum_at_owner(): lax.all_to_all(blocks, axis, split_axis=0, concat_axis=0, tiled=True)]
    all_gather x1 -> x0, blocking collectives: 15.7 us -> none  [whole_of(): x = lax.all_gather(x, axis, axis=dim, tiled=True)]
    all_to_all x2 -> x0, starting transfers between devices: 13.2 us -> none  [turned_blocks(): out = lax.all_to_all(out, axes[k], k, k, tiled=True)]
    all_to_all x2 -> x0, waiting for transfers between devices: 9.24 us -> none  [turned_blocks(): out = lax.all_to_all(out, axes[k], k, k, tiled=True)]
  transfers between devices with their start and end apart: 4 -> 0, of which waited for: 4 -> 0; matrix products, arithmetic and copies ran while one was open for 19% -> 0% of each run, Pallas kernels for 0% -> 0%
where the time goes in v1:
time: 96.1 us; the launch traced here: 95.8 us
  Pallas kernels  89 us (93%)
  local copies, waits for them, and re-layouts  4.69 us (5%)
  other arithmetic  1.48 us (2%)
    pallas_call x1, Pallas kernels, inproj(): pl.pallas_call(inproj_kernel, name='inproj', out_shape=(jax.ShapeDtypeStr...  56.7 us
    pallas_call x1, Pallas kernels, outproj(): pl.pallas_call(outproj_kernel, name='outproj', out_shape=jax.ShapeDtypeSt...  27 us
    pallas_call x1, Pallas kernels, mix(): pl.pallas_call(mix_kernel, name='mix', out_shape=(jax.ShapeDtypeStruct((N...  5.29 us

profile of v1, /device:TPU:1, one launch (start us, length us, event | category | flops | bytes accessed | tf_op | source)
XLA Modules:
  0.0 95.8 jit_solution(9130460965678652680)
XLA Ops:
  0.6 0.0 copy-start
  0.7 0.7 iota_add_fusion
  1.4 0.3 copy-done
  1.7 0.7 stack_broadcast_in_dim.7
  2.4 0.1 stack_broadcast_in_dim.8
  2.4 0.8 fusion.2
  3.2 0.1 copy.48
  3.3 0.1 stack.18
  3.4 0.1 copy.46
  3.5 0.1 stack.16
  3.5 0.1 copy.45
  3.6 0.1 stack.15
  3.7 0.1 copy.47
  3.8 0.1 stack.17
  3.9 0.7 copy.49.idx
  4.6 0.7 pad.4.wr
  5.3 56.7 %inproj.1 = (bf16[96,1536]{1,0:T(8,128)(2,1)}, f32[96,128]{1,0:T(8,128)}, bf16[8,512,128]{2,1,0:T(8,128)(2,1)}) custom-call(bf16[12,8,4,8,128]{4,3,2,1,0:T(8,128)(2,1)} %bitcast.51, bf16[128,512]{1,0:T(8,128)(2,1)} %wx.1, bf16[128,512]{1,0:T(8,128)(2,1)} %wz.1, bf16[128,256]{1,0:T(8,128)(2,1)} %wb.1, bf16[128,256]{1,0:T(8,128)(2,1)} %wc.1, ...), custom_call_target="tpu_custom_call" | custom-call | tf_op jit(solution)/shard_map/inproj/pallas_call | solution.py:282
  62.0 5.3 %mix.1 = (bf16[96,512]{1,0:T(8,128)(2,1)}, f32[8,512,128]{2,1,0:T(8,128)}) custom-call(s32[96,5]{1,0:T(8,128)} %copy.49.idx, bf16[96,1536]{1,0:T(8,128)(2,1)} %get-tuple-element.7.rows, f32[96,128]{1,0:T(8,128)} %get-tuple-element.8.aux, bf16[24,512]{1,0:T(8,128)(2,1)} %bitcast.54, bf16[48,512]{1,0:T(8,128)(2,1)} %bitcast.53, bf16[24,256]{1,0:T(8,128)(2,1)} %bitcast.58, ...), custom_call_target="tpu_custom_call" | custom-call | tf_op jit(solution)/shard_map/mix/pallas_call | solution.py:468
  67.3 27.0 %outproj.1 = bf16[96,512]{1,0:T(8,128)(2,1)} custom-call(bf16[96,512]{1,0:T(8,128)(2,1)} %get-tuple-element.9.gated, bf16[8,512,128]{2,1,0:T(8,128)(2,1)} %get-tuple-element.10.wog), custom_call_target="tpu_custom_call" | custom-call | tf_op jit(solution)/shard_map/outproj/pallas_call | solution.py:550
  94.3 1.5 %copy.51 = bf16[8,12,512]{2,0,1:T(8,128)(2,1)} copy(bf16[8,12,512]{2,0,1:T(8,128)(2,1)} %bitcast.52) | data formatting | bytes 196608
  (2 shorter events, 0.0 us)
Async XLA Ops:
  0.6 1.1 %copy-start = (bf16[4096,64]{0,1:T(8,128)(2,1)S(1)}, bf16[4096,64]{0,1:T(8,128)(2,1)}, u32[]{:S(2)}) copy-start(bf16[4096,64]{0,1:T(8,128)(2,1)} %param.41) | copy-start | bytes 1572868

commit v2 on v1

v2 whole, which is shorter than its diff:
```python
import functools

import jax
import jax.numpy as jnp
from jax import lax
from jax.experimental import pallas as pl
from jax.experimental.pallas import tpu as pltpu
from jax.sharding import Mesh
from jax.sharding import PartitionSpec as P

NZ, NX, NY, NC = 8, 4, 4, 2
NT = NY * NC
MESH = pl.DeviceIdType.MESH
KV = ("z", "x")
TP = ("y", "c")
EPS = 1e-06
HIGH = lax.Precision.HIGHEST
F32 = jnp.float32
BF16 = jnp.bfloat16
NQ, NS, NP, NH = 12, 8, 6, 8
VMEM_LIMIT = 60 * 1024 * 1024


def wrap(i, n):
    return lax.rem(i + n, n)


def remote(src, dst, send_sem, recv_sem, device):
    return pltpu.make_async_remote_copy(
        src_ref=src,
        dst_ref=dst,
        send_sem=send_sem,
        recv_sem=recv_sem,
        device_id=device,
        device_id_type=MESH,
    )


def greet(devices):
    barrier = pltpu.get_barrier_semaphore()
    for device in devices:
        pl.semaphore_signal(barrier, inc=1, device_id=device, device_id_type=MESH)
    pl.semaphore_wait(barrier, len(devices))


def hops_of(piece, way):
    return 4 if (piece % 2 == 0) == (way == 0) else 3


def silu(v):
    return v * (1.0 / (1.0 + jnp.exp(-v)))


def softplus(v):
    return jnp.maximum(v, 0.0) + jnp.log1p(jnp.exp(-jnp.abs(v)))


def iota(shape, dim):
    return lax.broadcasted_iota(jnp.int32, shape, dim)


def dot(a, b):
    return jnp.dot(a.astype(BF16), b.astype(BF16), preferred_element_type=F32)


def dot_of(a, b, dims, precision=None):
    return lax.dot_general(
        a, b, ((dims[:1], dims[1:]), ((), ())), precision=precision, preferred_element_type=F32
    )


def past(first, last):
    return jnp.concatenate([first[...].astype(F32), last[...].astype(F32)], axis=0)


def widen(v):
    spread = (iota((NH, 512), 1) // 64 == iota((NH, 512), 0)).astype(F32)
    return dot_of(v, spread, (1, 0), HIGH)


def upright(row):
    wide = jnp.broadcast_to(row[...].astype(F32), (NS, NS))
    return jnp.sum(
        jnp.where(iota((NS, NS), 0) == iota((NS, NS), 1), wide, 0.0), axis=1, keepdims=True
    )


def replay_kernel(
    accepted, cx, px, cb, pb, pdt, state, bias, alog, wtx, wtb, new_state, fresh_b, held, in_s, out_s
):
    def load(s):
        return pltpu.make_async_copy(state.at[s], held.at[s], in_s.at[s])

    def save(s):
        return pltpu.make_async_copy(held.at[s], new_state.at[s], out_s.at[s])

    for s in range(NS):
        load(s).start()

    def window(history, taps):
        summed = taps[0:1] * history[0 : NP * NS]
        for k in (1, 2, 3):
            summed = summed + taps[k : k + 1] * history[k * NS : (k + NP) * NS]
        return silu(summed)

    rate = -jnp.exp(alog[...])
    path_xs = window(past(cx, px), wtx[...].astype(F32))
    path_bs = window(past(cb, pb), wtb[...].astype(F32))
    path_step = softplus(pdt[...].astype(F32) + bias[...])
    count = jnp.concatenate([upright(accepted)] * NP, axis=0)
    live = ((iota((NP * NS, 1), 0) // NS).astype(F32) < count).astype(F32)
    path_log = path_step * rate * live
    tails = [jnp.zeros((NS, NH), F32)]
    for j in range(NP - 1, 0, -1):
        tails.insert(0, tails[0] + path_log[j * NS : (j + 1) * NS])
    overall = jnp.exp(tails[0] + path_log[0:NS])
    weights = live * jnp.exp(jnp.concatenate(tails, axis=0)) * path_step
    weighted = (path_xs * widen(weights)).astype(BF16)
    path_seq = lax.rem(iota((NP * NS, 128), 0), NS)
    gained = []
    for g in range(2):
        split_b = jnp.concatenate(
            [
                jnp.where(path_seq == s, path_bs[:, 128 * g : 128 * g + 128], 0.0)
                for s in range(NS)
            ],
            axis=1,
        ).astype(BF16)
        gained.append(dot_of(weighted[:, 256 * g : 256 * g + 256], split_b, (0, 0)))
    for s in range(NS):
        load(s).wait()
        at = slice(128 * s, 128 * s + 128)
        for g in range(2):
            wide = slice(256 * g, 256 * g + 256)
            fade = jnp.concatenate(
                [
                    jnp.broadcast_to(overall[s : s + 1, h : h + 1], (64, 128))
                    for h in range(4 * g, 4 * g + 4)
                ],
                axis=0,
            )
            fresh = fade * held[s, wide, :] + gained[g][:, at]
            held[s, wide, :] = fresh
            fresh_b[g, :, at] = fresh.astype(BF16)
        save(s).start()
    for s in range(NS):
        save(s).wait()


def replay(*args):
    vmem = pl.BlockSpec(memory_space=pltpu.VMEM)
    far = pl.BlockSpec(memory_space=pl.ANY)
    return pl.pallas_call(
        replay_kernel,
        name="replay",
        out_shape=(
            jax.ShapeDtypeStruct((NS, 512, 128), F32),
            jax.ShapeDtypeStruct((2, 256, 1024), BF16),
        ),
        in_specs=[vmem] * 6 + [far] + [vmem] * 4,
        out_specs=(far, vmem),
        scratch_shapes=[
            pltpu.VMEM((NS, 512, 128), F32),
            pltpu.SemaphoreType.DMA((NS,)),
            pltpu.SemaphoreType.DMA((NS,)),
        ],
        compiler_params=pltpu.CompilerParams(vmem_limit_bytes=VMEM_LIMIT),
    )(*args)


def mixer_kernel(
    tok_h,
    wx_h,
    wz_h,
    wb_h,
    wc_h,
    wdt_h,
    wo_h,
    fresh_h,
    gain,
    parents,
    accepted,
    cx,
    px,
    cb,
    pb,
    cc,
    pc,
    bias,
    alog,
    dskip,
    wtx,
    wtb,
    wtc,
    gain_out,
    mixed,
    tok,
    wown,
    wr,
    wo,
    fresh,
    tg,
    ts,
    wg,
    wog,
    prod,
    aprod,
    ring,
    aring,
    stage,
    astage,
    gated,
    gg,
    woc,
    kept,
    given,
    taken,
    part,
    terms,
    l_s,
    t_s,
    t_r,
    f_s,
    f_r,
    w_s,
    w_r,
    r_s,
    r_r,
    o_s,
    o_r,
    g_s,
    g_r,
    d_s,
    d_r,
    p_s,
    p_r,
):
    z, x = lax.axis_index("z"), lax.axis_index("x")
    y, c = lax.axis_index("y"), lax.axis_index("c")
    t = y * NC + c
    count = NQ * NS

    def depth_of(owner):
        return pl.ds(pl.multiple_of(owner * 128, 128), 128)

    sources = [
        wx_h.at[:, 0:256],
        wx_h.at[:, 256:512],
        wb_h,
        wc_h,
        wz_h.at[:, 0:256],
        wz_h.at[:, 256:512],
    ]
    loads = [(tok_h, tok)] + [(sources[p], wown.at[p]) for p in range(6)]
    loads.append((wo_h, wo))
    loads.append(
        (
            wdt_h.at[
                pl.ds(pl.multiple_of(t * NH, NH), NH), pl.ds(pl.multiple_of(z * 512, 512), 512)
            ],
            wr,
        )
    )
    loads.append((fresh_h, fresh))

    def load(k):
        return pltpu.make_async_copy(loads[k][0], loads[k][1], l_s.at[k])

    for k in range(len(loads)):
        load(k).start()
    plane = [(d, e) for d in range(NX) for e in range(NY) if d + e > 0]
    greet(
        [{"x": wrap(x + d, NX), "y": wrap(y + e, NY)} for d, e in plane]
        + [{"z": wrap(z + 1, NZ)}, {"z": wrap(z - 1, NZ)}, {"c": 1 - c}]
    )
    half = pl.ds(4 * c, 4)

    def tok_copy(d):
        to = wrap(x + d, NX)
        return remote(
            tok.at[:, half, to], tg.at[x, :, half], t_s.at[d - 1], t_r.at[d - 1], {"x": to}
        )

    def tok_share(d):
        block = tg.at[wrap(x - d, NX), :, half]
        return remote(block, block, f_s.at[d - 1], f_r.at[d - 1], {"c": 1 - c})

    def w_own(p, way):
        to = wrap(x + (1 if way == 0 else -1), NX)
        return remote(
            wown.at[p], wg.at[p, depth_of(x), :], w_s.at[p, way], w_r.at[p, way], {"x": to}
        )

    def w_pass(p):
        sign = 1 if p % 2 == 0 else -1
        block = wg.at[p, depth_of(wrap(x - sign, NX)), :]
        return remote(block, block, w_s.at[p, 2], w_r.at[p, 2], {"x": wrap(x + sign, NX)})

    def o_copy(way, hop):
        sign = 1 if way == 0 else -1
        owner = wrap(z - sign * (hop - 1), NZ)
        src = wo if hop == 1 else wog.at[owner]
        dst = wog.at[owner]
        if hop == 4:
            src, dst = src.at[pl.ds(256 * way, 256)], dst.at[pl.ds(256 * way, 256)]
        return remote(
            src, dst, o_s.at[way, hop - 1], o_r.at[way, hop - 1], {"z": wrap(z + sign, NZ)}
        )

    def r_copy(p, way, hop):
        to = {"z": wrap(z + (1 if way == 0 else -1), NZ)}
        if p == 6:
            src = astage.at[way] if hop == 1 else aring.at[way, hop - 2]
            dst = aring.at[way, hop - 1]
        else:
            src = stage.at[p, way] if hop == 1 else ring.at[p, way, hop - 2]
            dst = ring.at[p, way, hop - 1]
        return remote(src, dst, r_s.at[p, way, hop - 1], r_r.at[p, way, hop - 1], to)

    def own_term(p, dest):
        if p == 6:
            return aprod[:, pl.ds(dest, 1)].reshape(NQ, NS, 128)
        return prod[p, :, pl.ds(dest, 1)].reshape(NQ, NS, 256)

    def r_step(p, hop):
        for way in (0, 1):
            hops = hops_of(p, way)
            if hop > hops:
                continue
            sign = 1 if way == 0 else -1
            term = own_term(p, wrap(z + sign * (hops + 1 - hop), NZ))
            if hop == 1:
                if p == 6:
                    astage[way] = term.astype(BF16)
                else:
                    stage[p, way] = term.astype(BF16)
            else:
                r_copy(p, way, hop - 1).wait_recv()
                if p == 6:
                    aring[way, hop - 2] = (aring[way, hop - 2].astype(F32) + term).astype(BF16)
                else:
                    ring[p, way, hop - 2] = (ring[p, way, hop - 2].astype(F32) + term).astype(BF16)
            r_copy(p, way, hop).start()

    def r_total(p):
        total = own_term(p, z)
        for way in (0, 1):
            hops = hops_of(p, way)
            r_copy(p, way, hops).wait_recv()
            arrived = aring[way, hops - 1] if p == 6 else ring[p, way, hops - 1]
            total = total + arrived.astype(F32)
        return total.reshape(count, total.shape[2])

    order = (2, 1, 3)
    load(0).wait()
    for d in order:
        tok_copy(d).start()

    def w_send(ch):
        for p in (2 * ch, 2 * ch + 1):
            load(1 + p).wait()
            w_own(p, p % 2).start()
            w_own(p, 1 - p % 2).start()

    def o_send(hop):
        for way in (0, 1):
            if hop > 1:
                o_copy(way, hop - 1).wait_recv()
            o_copy(way, hop).start()

    w_send(0)
    w_send(1)
    load(7).wait()
    o_send(1)
    load(6).wait()
    load(5).wait()
    load(8).wait()
    load(9).wait()
    tg[pl.ds(x, 1)] = tok[:, :, pl.ds(x, 1)].reshape(1, NQ, NZ, NS, 128)
    for p in range(6):
        wg[p, depth_of(x), :] = wown[p]
    wog[pl.ds(z, 1)] = wo[...].reshape(1, 512, 128)

    up = jnp.concatenate([parents[:, q : q + 1] for q in range(NQ)], axis=0).astype(F32)
    taken_in = jnp.concatenate([upright(accepted)] * NQ, axis=0)
    seq = lax.rem(iota((count, 1), 0), NS).astype(F32)
    is_root = up < 0.0
    nodes = iota((count, 9 * NS + count), 1).astype(F32)

    def reach(back, other):
        return jnp.where(is_root, (taken_in + back) * NS + seq, other)

    at_kin = up * NS + seq
    kin = iota((count, count), 1).astype(F32)
    links = (kin == jnp.where(is_root, -1.0, at_kin)).astype(F32)
    eye = (iota((count, count), 0) == iota((count, count), 1)).astype(F32)
    family = eye + links
    for _ in range(4):
        family = jnp.minimum(dot(family, family), 1.0)
    is_kin = family > 0.5
    one = (nodes == reach(2.0, 9.0 * NS + at_kin)).astype(F32)
    two = dot(links, one) + (nodes == reach(1.0, -1.0)).astype(F32)
    three = dot(links, two) + (nodes == reach(0.0, -1.0)).astype(F32)
    one, two, three = one.astype(BF16), two.astype(BF16), three.astype(BF16)

    def tree_conv(first, last, own, taps):
        values = jnp.concatenate([past(first, last), own], axis=0).astype(BF16)
        summed = taps[3:4] * own
        for k, far in ((2, one), (1, two), (0, three)):
            summed = summed + taps[k : k + 1] * dot(far, values)
        return silu(summed)

    for d in order:
        tok_copy(d).wait_recv()
        tok_share(d).start()
    o_send(2)

    def forward(ch):
        for p in (2 * ch, 2 * ch + 1):
            w_own(p, p % 2).wait_recv()
            w_pass(p).start()

    def multiply(ch):
        for p in (2 * ch, 2 * ch + 1):
            w_own(p, 1 - p % 2).wait_recv()
            w_pass(p).wait_recv()
            prod[p] = jnp.dot(ts[...], wg[p], preferred_element_type=F32).reshape(
                NQ, NZ, NS, 256
            )
            r_step(p, 1)

    def advance(ch, hop):
        for p in (2 * ch, 2 * ch + 1):
            r_step(p, hop)

    forward(0)
    w_own(4, 0).start()
    w_own(4, 1).start()
    w_own(5, 1).start()
    w_own(5, 0).start()
    for d in order:
        tok_share(d).wait_recv()
    squares = jnp.zeros((NQ * NZ * NS, 128), F32)
    for xs in range(NX):
        values = tg[xs].reshape(NQ * NZ * NS, 128).astype(F32)
        squares = squares + values * values
        ts[:, xs * 128 : (xs + 1) * 128] = (values * gain[pl.ds(z * NX + xs, 1), :]).astype(BF16)
    lane = iota((NQ * NZ * NS, 128), 1)
    tall = jnp.concatenate([wr[...].astype(F32), jnp.zeros((120, 512), F32)], axis=0).astype(BF16)
    rates = dot_of(ts[...], tall, (1, 1))
    sums = jnp.sum(squares, axis=1, keepdims=True)
    aprod[...] = jnp.where(lane == 8, sums, rates).reshape(NQ, NZ, NS, 128)
    r_step(6, 1)
    multiply(0)
    forward(1)
    o_send(3)
    r_step(6, 2)
    advance(0, 2)
    multiply(1)
    forward(2)
    r_step(6, 3)
    advance(0, 3)
    advance(1, 2)
    multiply(2)
    o_send(4)
    r_step(6, 4)
    advance(0, 4)
    advance(1, 3)
    advance(2, 2)

    total = r_total(6)
    scale = lax.rsqrt(total[:, 8:9] / (NZ * NX * 128.0) + EPS)
    rate = -jnp.exp(alog[...])
    step = softplus((total[:, 0:NH] * scale).astype(BF16).astype(F32) + bias[...])
    slope = step * rate
    decay = dot_of(family, slope, (1, 0), HIGH)
    decay_t = dot_of(slope, family, (0, 1), HIGH)
    step_t = dot_of(step, eye, (0, 1), HIGH)
    grown = widen(jnp.exp(decay))
    skip = widen(jnp.broadcast_to(dskip[...], (NS, NH)))[0:1]

    def scaled_rows(p):
        return (r_total(p) * scale).astype(BF16).astype(F32)

    advance(1, 4)
    advance(2, 3)
    post_x = tree_conv(
        cx,
        px,
        jnp.concatenate([scaled_rows(0), scaled_rows(1)], axis=1),
        wtx[...].astype(F32),
    )
    post_xb = post_x.astype(BF16)
    advance(2, 4)
    post_b = tree_conv(cb, pb, scaled_rows(2), wtb[...].astype(F32)).astype(BF16)
    post_c = tree_conv(cc, pc, scaled_rows(3), wtc[...].astype(F32)).astype(BF16)
    seq_of = lax.rem(iota((count, 128), 0), NS)
    side = iota((count, 128), 1)
    heads_of = []
    for g in range(2):
        wide, narrow = slice(256 * g, 256 * g + 256), slice(128 * g, 128 * g + 128)
        post_bg, post_cg = post_b[:, narrow], post_c[:, narrow]
        split_c = jnp.concatenate(
            [jnp.where(seq_of == s, post_cg.astype(F32), 0.0) for s in range(NS)], axis=1
        ).astype(BF16)
        carried = dot_of(split_c, fresh[g], (1, 1))
        scores = dot_of(post_cg, post_bg, (1, 1))
        within = []
        for pair in range(2):
            sides = []
            at = 256 * g + 128 * pair
            for h in (4 * g + 2 * pair, 4 * g + 2 * pair + 1):
                gap = decay[:, h : h + 1] - decay_t[h : h + 1, :]
                mixing = jnp.exp(jnp.where(is_kin, gap, 0.0)) * step_t[h : h + 1, :]
                mixing = jnp.where(is_kin, scores * mixing, 0.0)
                sides.append(dot(mixing, post_xb[:, at : at + 128]))
            within.append(jnp.where(side < 64, sides[0], sides[1]))
        heads = carried * grown[:, wide] + jnp.concatenate(within, axis=1)
        heads_of.append(heads + skip[:, wide] * post_x[:, wide])
    for way in (0, 1):
        o_copy(way, 4).wait_recv()
    for k in range(NZ):
        at = 512 * (k % 2) + 128 * (k // 2)
        woc[:, at : at + 128] = wog[k]
    for g in range(2):
        wide = slice(256 * g, 256 * g + 256)
        heads = heads_of[g] * silu(scaled_rows(4 + g))
        spread_of = jnp.sum(heads * heads, axis=1, keepdims=True) / 256.0
        heads = heads * lax.rsqrt(spread_of + EPS) * gain_out[:, wide]
        gated[:, wide] = heads.astype(BF16)

    def g_copy(d):
        return remote(
            gated, gg.at[d - 1], g_s.at[d - 1], g_r.at[d - 1], {"x": wrap(x + d, NX)}
        )

    def d_copy(d):
        return remote(given.at[d], taken.at[d], d_s.at[d], d_r.at[d], {"c": 1 - c})

    def p_copy(d, e):
        to_y = wrap(y + e, NY)
        return remote(
            part.at[d, to_y],
            terms.at[x * NY + y],
            p_s.at[d, e],
            p_r.at[d, e],
            {"x": wrap(x - d, NX), "y": to_y},
        )

    for d in order:
        g_copy(d).start()

    def product(d):
        if d > 0:
            g_copy(d).wait_recv()
        values = gated[...] if d == 0 else gg[d - 1]
        mine = pl.ds(pl.multiple_of(512 * c, 512), 512)
        other = pl.ds(pl.multiple_of(512 * (1 - c), 512), 512)
        given[d] = jnp.dot(values, woc[:, other], preferred_element_type=F32).astype(BF16)
        d_copy(d).start()
        kept[d] = jnp.dot(values, woc[:, mine], preferred_element_type=F32)

    def deliver(d):
        d_copy(d).wait_recv()
        both = (kept[d] + taken[d].astype(F32)).astype(BF16)
        for to in range(NY):
            part[d, to] = both[:, 128 * to : 128 * to + 128]
        for e in (2, 1, 3, 0):
            if d + e > 0:
                p_copy(d, e).start()

    product(0)
    deliver(0)
    terms[pl.ds(x * NY + y, 1)] = part[0, pl.ds(y, 1)]
    product(2)
    deliver(2)
    product(1)
    product(3)
    deliver(1)
    deliver(3)
    for d, e in plane:
        p_copy(d, e).wait_recv()
    for xs in range(NX):
        total = terms[xs * NY].astype(F32)
        for k in range(1, NY):
            total = total + terms[xs * NY + k].astype(F32)
        mixed[:, xs * 128 : (xs + 1) * 128] = total

    for way in (0, 1):
        for hop in (1, 2, 3, 4):
            o_copy(way, hop).wait_send()
    for d in order:
        tok_copy(d).wait_send()
        tok_share(d).wait_send()
        g_copy(d).wait_send()
    for p in range(6):
        w_own(p, 0).wait_send()
        w_own(p, 1).wait_send()
        w_pass(p).wait_send()
    for p in range(7):
        for way in (0, 1):
            for hop in range(1, hops_of(p, way) + 1):
                r_copy(p, way, hop).wait_send()
    for d in range(NX):
        d_copy(d).wait_send()
    for d, e in plane:
        p_copy(d, e).wait_send()


def mixer(*args):
    vmem = pl.BlockSpec(memory_space=pltpu.VMEM)
    far = pl.BlockSpec(memory_space=pl.ANY)
    dma = pltpu.SemaphoreType.DMA
    rows = NQ * NS
    return pl.pallas_call(
        mixer_kernel,
        name="mixer",
        out_shape=jax.ShapeDtypeStruct((rows, 512), F32),
        in_specs=[far] * 8 + [vmem] * (len(args) - 8),
        out_specs=vmem,
        scratch_shapes=[
            pltpu.VMEM((NQ, NZ, NX, NS, 128), BF16),
            pltpu.VMEM((6, 128, 256), BF16),
            pltpu.VMEM((NH, 512), BF16),
            pltpu.VMEM((512, 128), BF16),
            pltpu.VMEM((2, 256, 1024), BF16),
            pltpu.VMEM((NX, NQ, NZ, NS, 128), BF16),
            pltpu.VMEM((NZ * rows, 512), BF16),
            pltpu.VMEM((6, 512, 256), BF16),
            pltpu.VMEM((NZ, 512, 128), BF16),
            pltpu.VMEM((6, NQ, NZ, NS, 256), F32),
            pltpu.VMEM((NQ, NZ, NS, 128), F32),
            pltpu.VMEM((6, 2, 4, NQ, NS, 256), BF16),
            pltpu.VMEM((2, 4, NQ, NS, 128), BF16),
            pltpu.VMEM((6, 2, NQ, NS, 256), BF16),
            pltpu.VMEM((2, NQ, NS, 128), BF16),
            pltpu.VMEM((rows, 512), BF16),
            pltpu.VMEM((3, rows, 512), BF16),
            pltpu.VMEM((512, 1024), BF16),
            pltpu.VMEM((NX, rows, 512), F32),
            pltpu.VMEM((NX, rows, 512), BF16),
            pltpu.VMEM((NX, rows, 512), BF16),
            pltpu.VMEM((NX, NY, rows, 128), BF16),
            pltpu.VMEM((NX * NY, rows, 128), BF16),
            dma((10,)),
            dma((3,)),
            dma((3,)),
            dma((3,)),
            dma((3,)),
            dma((6, 3)),
            dma((6, 3)),
            dma((7, 2, 4)),
            dma((7, 2, 4)),
            dma((2, 4)),
            dma((2, 4)),
            dma((3,)),
            dma((3,)),
            dma((NX,)),
            dma((NX,)),
            dma((NX, NY)),
            dma((NX, NY)),
        ],
        compiler_params=pltpu.CompilerParams(
            collective_id=0, has_side_effects=True, vmem_limit_bytes=VMEM_LIMIT
        ),
    )(*args)


def by_place(v):
    v = jnp.transpose(v, (1, 0, 2))
    return v.reshape(v.shape[0] * v.shape[1], v.shape[2])


def shards(
    tokens,
    parents,
    accepted,
    state,
    conv_x,
    conv_b,
    conv_c,
    path_x,
    path_b,
    path_c,
    path_dt,
    gain_in,
    w_x,
    w_z,
    w_b,
    w_c,
    w_dt,
    dt_bias,
    a_log,
    d_skip,
    conv_wx,
    conv_wb,
    conv_wc,
    gain_out,
    w_out,
):
    tok = jnp.transpose(tokens, (1, 0, 2)).reshape(NQ, NZ, NX, NS, 128)
    conv_x, path_x = by_place(conv_x), by_place(path_x)
    conv_b, path_b = by_place(conv_b), by_place(path_b)
    conv_c, path_c = by_place(conv_c), by_place(path_c)
    accepted, dt_bias, a_log = accepted[None, :], dt_bias[None, :], a_log[None, :]
    new_state, fresh = replay(
        accepted,
        conv_x,
        path_x,
        conv_b,
        path_b,
        by_place(path_dt),
        state.reshape(NS, 512, 128),
        dt_bias,
        a_log,
        conv_wx,
        conv_wb,
    )
    mixed = mixer(
        tok,
        w_x,
        w_z,
        w_b,
        w_c,
        w_dt.T,
        w_out,
        fresh,
        gain_in.reshape(32, 128),
        parents,
        accepted,
        conv_x,
        path_x,
        conv_b,
        path_b,
        conv_c,
        path_c,
        dt_bias,
        a_log,
        d_skip[None, :],
        conv_wx,
        conv_wb,
        conv_wc,
        gain_out[None, :],
    )
    mixed = jnp.transpose(mixed.reshape(NQ, NS, 512).astype(BF16), (1, 0, 2))
    return (mixed, new_state.reshape(NS, NH, 64, 128))


def solution(mesh):
    finer = Mesh(mesh.devices.reshape(NZ, NX, NY, NC), ("z", "x", "y", "c"))
    return jax.shard_map(
        shards,
        mesh=finer,
        in_specs=(
            P(None, None, KV),
            P(KV, None),
            P(KV),
            P(KV, TP, None, None),
            P(KV, None, TP),
            P(KV, None, TP),
            P(KV, None, TP),
            P(KV, None, TP),
            P(KV, None, TP),
            P(KV, None, TP),
            P(KV, None, TP),
            P(),
            P(KV, TP),
            P(KV, TP),
            P(KV, TP),
            P(KV, TP),
            P(),
            P(TP),
            P(TP),
            P(TP),
            P(None, TP),
            P(None, TP),
            P(None, TP),
            P(TP),
            P(TP, KV),
        ),
        out_specs=(P(KV, None, TP), P(KV, TP, None, None)),
        check_vma=False,
    )
```

time: 96.1 us -> 80.1 us (0.83)
  Pallas kernels: 89 us -> 77.6 us
  local copies, waits for them, and re-layouts: 4.69 us -> 0 us
    pallas_call x3 -> x2, Pallas kernels: 89 us -> 77.6 us  [the longest x1 72.7 us: mixer(): pl.pallas_call(mixer_kernel, name='mixer', out_shape=jax.ShapeDtypeStruct...]
    unnamed x3 -> x0, local copies, waits for them, and re-layouts: 1.87 us -> none
    another operation x8 -> x0, local copies, waits for them, and re-layouts: 1.82 us -> none  [shards(): jnp.stack([jnp.where(root, (acc + 2) * NS + seq, 9 * NS + up * NS + seq),...]
    transpose x0 -> x1, other arithmetic: none -> 1.58 us  [shards(): mixed = jnp.transpose(mixed.reshape(NQ, NS, 512).astype(BF16), (1, 0, 2))]
where the time goes in v2:
time: 80.1 us; the launch traced here: 79.8 us
  Pallas kernels  77.6 us (97%)
  other arithmetic  1.58 us (2%)
    pallas_call x1, Pallas kernels, mixer(): pl.pallas_call(mixer_kernel, name='mixer', out_shape=jax.ShapeDtypeStruct...  72.7 us
    pallas_call x1, Pallas kernels, replay(): pl.pallas_call(replay_kernel, name='replay', out_shape=(jax.ShapeDtypeStr...  4.86 us

profile of v2, /device:TPU:1, one launch (start us, length us, event | category | flops | bytes accessed | tf_op | source)
XLA Modules:
  0.0 79.8 jit_solution(9292579739771634999)
XLA Ops:
  0.6 4.9 %replay.1 = (f32[8,512,128]{2,1,0:T(8,128)}, bf16[2,256,1024]{2,1,0:T(8,128)(2,1)}) custom-call(s32[1,8]{1,0:T(1,128)} %bitcast.53, bf16[24,512]{1,0:T(8,128)(2,1)} %bitcast.42, bf16[48,512]{1,0:T(8,128)(2,1)} %bitcast.40, bf16[24,256]{1,0:T(8,128)(2,1)} %bitcast.46, bf16[48,256]{1,0:T(8,128)(2,1)} %bitcast.44, bf16[48,8]{1,0:T(8,128)(2,1)} %bitcast.50, ...), custom_call_target="tpu_custom_call" | custom-call | tf_op jit(solution)/shard_map/replay/pallas_call | solution.py:153
  5.5 72.7 %mixer.1 = f32[96,512]{1,0:T(8,128)} custom-call(bf16[12,8,4,8,128]{4,3,2,1,0:T(8,128)(2,1)} %bitcast.38, bf16[128,512]{1,0:T(8,128)(2,1)} %wx_h.1, bf16[128,512]{1,0:T(8,128)(2,1)} %wz_h.1, bf16[128,256]{1,0:T(8,128)(2,1)} %wb_h.1, bf16[128,256]{1,0:T(8,128)(2,1)} %wc_h.1, bf16[64,4096]{1,0:T(8,128)(2,1)} %bitcast.39, bf16[512,128]{1,0:T(8,128)(2,1)} %wo_h.1, ...), custom_call_target="tpu_custom_call" | custom-call | tf_op jit(solution)/shard_map/mixer/pallas_call | solution.py:615
  78.2 1.6 %convert_bitcast_fusion = bf16[8,12,512]{2,0,1:T(8,128)(2,1)} fusion(f32[96,512]{1,0:T(8,128)} %mixer.1), kind=kLoop, calls=%fused_computation | loop fusion | flops 49152 | bytes 294912 | tf_op jit(solution)/shard_map/transpose | solution.py:745

commit v3 on v2

--- a/solution.py
+++ b/solution.py
@@ -85,89 +85,6 @@
     )
 
 
-def replay_kernel(
-    accepted, cx, px, cb, pb, pdt, state, bias, alog, wtx, wtb, new_state, fresh_b, held, in_s, out_s
-):
-    def load(s):
-        return pltpu.make_async_copy(state.at[s], held.at[s], in_s.at[s])
-
-    def save(s):
-        return pltpu.make_async_copy(held.at[s], new_state.at[s], out_s.at[s])
-
-    for s in range(NS):
-        load(s).start()
-
-    def window(history, taps):
-        summed = taps[0:1] * history[0 : NP * NS]
-        for k in (1, 2, 3):
-            summed = summed + taps[k : k + 1] * history[k * NS : (k + NP) * NS]
-        return silu(summed)
-
-    rate = -jnp.exp(alog[...])
-    path_xs = window(past(cx, px), wtx[...].astype(F32))
-    path_bs = window(past(cb, pb), wtb[...].astype(F32))
-    path_step = softplus(pdt[...].astype(F32) + bias[...])
-    count = jnp.concatenate([upright(accepted)] * NP, axis=0)
-    live = ((iota((NP * NS, 1), 0) // NS).astype(F32) < count).astype(F32)
-    path_log = path_step * rate * live
-    tails = [jnp.zeros((NS, NH), F32)]
-    for j in range(NP - 1, 0, -1):
-        tails.insert(0, tails[0] + path_log[j * NS : (j + 1) * NS])
-    overall = jnp.exp(tails[0] + path_log[0:NS])
-    weights = live * jnp.exp(jnp.concatenate(tails, axis=0)) * path_step
-    weighted = (path_xs * widen(weights)).astype(BF16)
-    path_seq = lax.rem(iota((NP * NS, 128), 0), NS)
-    gained = []
-    for g in range(2):
-        split_b = jnp.concatenate(
-            [
-                jnp.where(path_seq == s, path_bs[:, 128 * g : 128 * g + 128], 0.0)
-                for s in range(NS)
-            ],
-            axis=1,
-        ).astype(BF16)
-        gained.append(dot_of(weighted[:, 256 * g : 256 * g + 256], split_b, (0, 0)))
-    for s in range(NS):
-        load(s).wait()
-        at = slice(128 * s, 128 * s + 128)
-        for g in range(2):
-            wide = slice(256 * g, 256 * g + 256)
-            fade = jnp.concatenate(
-                [
-                    jnp.broadcast_to(overall[s : s + 1, h : h + 1], (64, 128))
-                    for h in range(4 * g, 4 * g + 4)
-                ],
-                axis=0,
-            )
-            fresh = fade * held[s, wide, :] + gained[g][:, at]
-            held[s, wide, :] = fresh
-            fresh_b[g, :, at] = fresh.astype(BF16)
-        save(s).start()
-    for s in range(NS):
-        save(s).wait()
-
-
-def replay(*args):
-    vmem = pl.BlockSpec(memory_space=pltpu.VMEM)
-    far = pl.BlockSpec(memory_space=pl.ANY)
-    return pl.pallas_call(
-        replay_kernel,
-        name="replay",
-        out_shape=(
-            jax.ShapeDtypeStruct((NS, 512, 128), F32),
-            jax.ShapeDtypeStruct((2, 256, 1024), BF16),
-        ),
-        in_specs=[vmem] * 6 + [far] + [vmem] * 4,
-        out_specs=(far, vmem),
-        scratch_shapes=[
-            pltpu.VMEM((NS, 512, 128), F32),
-            pltpu.SemaphoreType.DMA((NS,)),
-            pltpu.SemaphoreType.DMA((NS,)),
-        ],
-        compiler_params=pltpu.CompilerParams(vmem_limit_bytes=VMEM_LIMIT),
-    )(*args)
-
-
 def mixer_kernel(
     tok_h,
     wx_h,
@@ -176,7 +93,7 @@
     wc_h,
     wdt_h,
     wo_h,
-    fresh_h,
+    state_h,
     gain,
     parents,
     accepted,
@@ -186,6 +103,7 @@
     pb,
     cc,
     pc,
+    pdt,
     bias,
     alog,
     dskip,
@@ -194,10 +112,12 @@
     wtc,
     gain_out,
     mixed,
+    new_state,
     tok,
     wown,
     wr,
     wo,
+    held,
     fresh,
     tg,
     ts,
@@ -218,6 +138,8 @@
     part,
     terms,
     l_s,
+    s_s,
+    n_s,
     t_s,
     t_r,
     f_s,
@@ -261,13 +183,20 @@
             wr,
         )
     )
-    loads.append((fresh_h, fresh))
 
     def load(k):
         return pltpu.make_async_copy(loads[k][0], loads[k][1], l_s.at[k])
 
-    for k in range(len(loads)):
+    def load_state(s):
+        return pltpu.make_async_copy(state_h.at[s], held.at[s], s_s.at[s])
+
+    def save_state(s):
+        return pltpu.make_async_copy(held.at[s], new_state.at[s], n_s.at[s])
+
+    for k in (1, 2, 0, 3, 4, 7, 5, 6, 8):
         load(k).start()
+    for s in range(NS):
+        load_state(s).start()
     plane = [(d, e) for d in range(NX) for e in range(NY) if d + e > 0]
     greet(
         [{"x": wrap(x + d, NX), "y": wrap(y + e, NY)} for d, e in plane]
@@ -319,7 +248,7 @@
 
     def own_term(p, dest):
         if p == 6:
-            return aprod[:, pl.ds(dest, 1)].reshape(NQ, NS, 128)
+            return aprod[pl.ds(dest, 1)].reshape(16, count)
         return prod[p, :, pl.ds(dest, 1)].reshape(NQ, NS, 256)
 
     def r_step(p, hop):
@@ -349,12 +278,9 @@
             r_copy(p, way, hops).wait_recv()
             arrived = aring[way, hops - 1] if p == 6 else ring[p, way, hops - 1]
             total = total + arrived.astype(F32)
-        return total.reshape(count, total.shape[2])
+        return total if p == 6 else total.reshape(count, 256)
 
     order = (2, 1, 3)
-    load(0).wait()
-    for d in order:
-        tok_copy(d).start()
 
     def w_send(ch):
         for p in (2 * ch, 2 * ch + 1):
@@ -369,17 +295,11 @@
             o_copy(way, hop).start()
 
     w_send(0)
-    w_send(1)
+    load(0).wait()
+    for d in order:
+        tok_copy(d).start()
     load(7).wait()
     o_send(1)
-    load(6).wait()
-    load(5).wait()
-    load(8).wait()
-    load(9).wait()
-    tg[pl.ds(x, 1)] = tok[:, :, pl.ds(x, 1)].reshape(1, NQ, NZ, NS, 128)
-    for p in range(6):
-        wg[p, depth_of(x), :] = wown[p]
-    wog[pl.ds(z, 1)] = wo[...].reshape(1, 512, 128)
 
     up = jnp.concatenate([parents[:, q : q + 1] for q in range(NQ)], axis=0).astype(F32)
     taken_in = jnp.concatenate([upright(accepted)] * NQ, axis=0)
@@ -403,6 +323,68 @@
     three = dot(links, two) + (nodes == reach(0.0, -1.0)).astype(F32)
     one, two, three = one.astype(BF16), two.astype(BF16), three.astype(BF16)
 
+    def window(history, taps):
+        summed = taps[0:1] * history[0 : NP * NS]
+        for k in (1, 2, 3):
+            summed = summed + taps[k : k + 1] * history[k * NS : (k + NP) * NS]
+        return silu(summed)
+
+    rate = -jnp.exp(alog[...])
+    path_xs = window(past(cx, px), wtx[...].astype(F32))
+    path_bs = window(past(cb, pb), wtb[...].astype(F32))
+    path_step = softplus(pdt[...].astype(F32) + bias[...])
+    live = ((iota((NP * NS, 1), 0) // NS).astype(F32) < taken_in[0 : NP * NS]).astype(F32)
+    path_log = path_step * rate * live
+    tails = [jnp.zeros((NS, NH), F32)]
+    for j in range(NP - 1, 0, -1):
+        tails.insert(0, tails[0] + path_log[j * NS : (j + 1) * NS])
+    overall = jnp.exp(tails[0] + path_log[0:NS])
+    weights = live * jnp.exp(jnp.concatenate(tails, axis=0)) * path_step
+    weighted = (path_xs * widen(weights)).astype(BF16)
+    path_seq = lax.rem(iota((NP * NS, 128), 0), NS)
+
+    def forward(ch):
+        for p in (2 * ch, 2 * ch + 1):
+            w_own(p, p % 2).wait_recv()
+            w_pass(p).start()
+
+    forward(0)
+    w_send(1)
+    w_send(2)
+    o_send(2)
+    tg[pl.ds(x, 1)] = tok[:, :, pl.ds(x, 1)].reshape(1, NQ, NZ, NS, 128)
+    for p in range(6):
+        wg[p, depth_of(x), :] = wown[p]
+    wog[pl.ds(z, 1)] = wo[...].reshape(1, 512, 128)
+    load(8).wait()
+
+    gained = []
+    for g in range(2):
+        split_b = jnp.concatenate(
+            [
+                jnp.where(path_seq == s, path_bs[:, 128 * g : 128 * g + 128], 0.0)
+                for s in range(NS)
+            ],
+            axis=1,
+        ).astype(BF16)
+        gained.append(dot_of(weighted[:, 256 * g : 256 * g + 256], split_b, (0, 0)))
+    for s in range(NS):
+        load_state(s).wait()
+        at = slice(128 * s, 128 * s + 128)
+        for g in range(2):
+            wide = slice(256 * g, 256 * g + 256)
+            fade = jnp.concatenate(
+                [
+                    jnp.broadcast_to(overall[s : s + 1, h : h + 1], (64, 128))
+                    for h in range(4 * g, 4 * g + 4)
+                ],
+                axis=0,
+            )
+            now = fade * held[s, wide, :] + gained[g][:, at]
+            held[s, wide, :] = now
+            fresh[g, :, at] = now.astype(BF16)
+        save_state(s).start()
+
     def tree_conv(first, last, own, taps):
         values = jnp.concatenate([past(first, last), own], axis=0).astype(BF16)
         summed = taps[3:4] * own
@@ -413,77 +395,70 @@
     for d in order:
         tok_copy(d).wait_recv()
         tok_share(d).start()
-    o_send(2)
-
-    def forward(ch):
-        for p in (2 * ch, 2 * ch + 1):
-            w_own(p, p % 2).wait_recv()
-            w_pass(p).start()
 
     def multiply(ch):
         for p in (2 * ch, 2 * ch + 1):
             w_own(p, 1 - p % 2).wait_recv()
             w_pass(p).wait_recv()
-            prod[p] = jnp.dot(ts[...], wg[p], preferred_element_type=F32).reshape(
-                NQ, NZ, NS, 256
-            )
+            prod[p] = jnp.dot(
+                ts[...].reshape(NQ * NZ * NS, 512), wg[p], preferred_element_type=F32
+            ).reshape(NQ, NZ, NS, 256)
             r_step(p, 1)
 
     def advance(ch, hop):
         for p in (2 * ch, 2 * ch + 1):
             r_step(p, hop)
 
-    forward(0)
-    w_own(4, 0).start()
-    w_own(4, 1).start()
-    w_own(5, 1).start()
-    w_own(5, 0).start()
-    for d in order:
-        tok_share(d).wait_recv()
     squares = jnp.zeros((NQ * NZ * NS, 128), F32)
-    for xs in range(NX):
-        values = tg[xs].reshape(NQ * NZ * NS, 128).astype(F32)
+    for d in (0,) + order:
+        if d > 0:
+            tok_share(d).wait_recv()
+        xs = wrap(x - d, NX)
+        values = tg[pl.ds(xs, 1)].reshape(NQ * NZ * NS, 128).astype(F32)
         squares = squares + values * values
-        ts[:, xs * 128 : (xs + 1) * 128] = (values * gain[pl.ds(z * NX + xs, 1), :]).astype(BF16)
-    lane = iota((NQ * NZ * NS, 128), 1)
-    tall = jnp.concatenate([wr[...].astype(F32), jnp.zeros((120, 512), F32)], axis=0).astype(BF16)
-    rates = dot_of(ts[...], tall, (1, 1))
-    sums = jnp.sum(squares, axis=1, keepdims=True)
-    aprod[...] = jnp.where(lane == 8, sums, rates).reshape(NQ, NZ, NS, 128)
+        scaled = (values * gain[pl.ds(z * NX + xs, 1), :]).astype(BF16)
+        ts[:, :, :, depth_of(xs)] = scaled.reshape(NQ, NZ, NS, 128)
+    multiply(0)
+    tall = jnp.concatenate([wr[...].astype(F32), jnp.zeros((8, 512), F32)], axis=0).astype(BF16)
+    squares = squares.reshape(NQ, NZ, NS, 128)
+    for dest in range(NZ):
+        rates = dot_of(tall, ts[:, dest].reshape(count, 512), (1, 1))
+        sums = dot_of(
+            jnp.ones((16, 128), F32), squares[:, dest].reshape(count, 128), (1, 1), HIGH
+        )
+        aprod[dest] = jnp.where(iota((16, count), 0) == NH, sums, rates)
     r_step(6, 1)
-    multiply(0)
+    o_send(3)
     forward(1)
-    o_send(3)
+    advance(0, 2)
     r_step(6, 2)
-    advance(0, 2)
+    forward(2)
+    o_send(4)
     multiply(1)
-    forward(2)
+    advance(0, 3)
     r_step(6, 3)
-    advance(0, 3)
+    multiply(2)
     advance(1, 2)
-    multiply(2)
-    o_send(4)
+    advance(0, 4)
     r_step(6, 4)
-    advance(0, 4)
+    advance(2, 2)
     advance(1, 3)
-    advance(2, 2)
 
     total = r_total(6)
-    scale = lax.rsqrt(total[:, 8:9] / (NZ * NX * 128.0) + EPS)
-    rate = -jnp.exp(alog[...])
-    step = softplus((total[:, 0:NH] * scale).astype(BF16).astype(F32) + bias[...])
-    slope = step * rate
-    decay = dot_of(family, slope, (1, 0), HIGH)
-    decay_t = dot_of(slope, family, (0, 1), HIGH)
-    step_t = dot_of(step, eye, (0, 1), HIGH)
+    scale = lax.rsqrt(dot_of(eye, total, (1, 1), HIGH)[:, NH : NH + 1] / (NZ * NX * 128.0) + EPS)
+    scale_t = lax.rsqrt(total[NH : NH + 1] / (NZ * NX * 128.0) + EPS)
+    step_t = softplus((total[0:NH] * scale_t).astype(BF16).astype(F32) + upright(bias))
+    slope_t = step_t * -jnp.exp(upright(alog))
+    decay = dot_of(family, slope_t, (1, 1), HIGH)
+    decay_t = dot_of(slope_t, family, (1, 1), HIGH)
     grown = widen(jnp.exp(decay))
     skip = widen(jnp.broadcast_to(dskip[...], (NS, NH)))[0:1]
 
     def scaled_rows(p):
         return (r_total(p) * scale).astype(BF16).astype(F32)
 
+    advance(2, 3)
     advance(1, 4)
-    advance(2, 3)
     post_x = tree_conv(
         cx,
         px,
@@ -586,6 +561,8 @@
             total = total + terms[xs * NY + k].astype(F32)
         mixed[:, xs * 128 : (xs + 1) * 128] = total
 
+    for s in range(NS):
+        save_state(s).wait()
     for way in (0, 1):
         for hop in (1, 2, 3, 4):
             o_copy(way, hop).wait_send()
@@ -615,25 +592,29 @@
     return pl.pallas_call(
         mixer_kernel,
         name="mixer",
-        out_shape=jax.ShapeDtypeStruct((rows, 512), F32),
+        out_shape=(
+            jax.ShapeDtypeStruct((rows, 512), F32),
+            jax.ShapeDtypeStruct((NS, 512, 128), F32),
+        ),
         in_specs=[far] * 8 + [vmem] * (len(args) - 8),
-        out_specs=vmem,
+        out_specs=(vmem, far),
         scratch_shapes=[
             pltpu.VMEM((NQ, NZ, NX, NS, 128), BF16),
             pltpu.VMEM((6, 128, 256), BF16),
             pltpu.VMEM((NH, 512), BF16),
             pltpu.VMEM((512, 128), BF16),
+            pltpu.VMEM((NS, 512, 128), F32),
             pltpu.VMEM((2, 256, 1024), BF16),
             pltpu.VMEM((NX, NQ, NZ, NS, 128), BF16),
-            pltpu.VMEM((NZ * rows, 512), BF16),
+            pltpu.VMEM((NQ, NZ, NS, 512), BF16),
             pltpu.VMEM((6, 512, 256), BF16),
             pltpu.VMEM((NZ, 512, 128), BF16),
             pltpu.VMEM((6, NQ, NZ, NS, 256), F32),
-            pltpu.VMEM((NQ, NZ, NS, 128), F32),
+            pltpu.VMEM((NZ, 16, rows), F32),
             pltpu.VMEM((6, 2, 4, NQ, NS, 256), BF16),
-            pltpu.VMEM((2, 4, NQ, NS, 128), BF16),
+            pltpu.VMEM((2, 4, 16, rows), BF16),
             pltpu.VMEM((6, 2, NQ, NS, 256), BF16),
-            pltpu.VMEM((2, NQ, NS, 128), BF16),
+            pltpu.VMEM((2, 16, rows), BF16),
             pltpu.VMEM((rows, 512), BF16),
             pltpu.VMEM((3, rows, 512), BF16),
             pltpu.VMEM((512, 1024), BF16),
@@ -642,7 +623,9 @@
             pltpu.VMEM((NX, rows, 512), BF16),
             pltpu.VMEM((NX, NY, rows, 128), BF16),
             pltpu.VMEM((NX * NY, rows, 128), BF16),
-            dma((10,)),
+            dma((9,)),
+            dma((NS,)),
+            dma((NS,)),
             dma((3,)),
             dma((3,)),
             dma((3,)),
@@ -703,20 +686,7 @@
     conv_b, path_b = by_place(conv_b), by_place(path_b)
     conv_c, path_c = by_place(conv_c), by_place(path_c)
     accepted, dt_bias, a_log = accepted[None, :], dt_bias[None, :], a_log[None, :]
-    new_state, fresh = replay(
-        accepted,
-        conv_x,
-        path_x,
-        conv_b,
-        path_b,
-        by_place(path_dt),
-        state.reshape(NS, 512, 128),
-        dt_bias,
-        a_log,
-        conv_wx,
-        conv_wb,
-    )
-    mixed = mixer(
+    mixed, new_state = mixer(
         tok,
         w_x,
         w_z,
@@ -724,7 +694,7 @@
         w_c,
         w_dt.T,
         w_out,
-        fresh,
+        state.reshape(NS, 512, 128),
         gain_in.reshape(32, 128),
         parents,
         accepted,
@@ -734,6 +704,7 @@
         path_b,
         conv_c,
         path_c,
+        by_place(path_dt),
         dt_bias,
         a_log,
         d_skip[None, :],

time: 80.1 us -> 75.4 us (0.941)
  Pallas kernels: 77.6 us -> 69.8 us
  local copies, waits for them, and re-layouts: 0 us -> 3.16 us
    pallas_call x2 -> x1, Pallas kernels: 77.6 us -> 69.8 us  [mixer(): pl.pallas_call(mixer_kernel, name='mixer', out_shape=(jax.ShapeDtypeStruc...]
    unnamed x0 -> x1, local copies, waits for them, and re-layouts: none -> 3.16 us
where the time goes in v3:
time: 75.4 us; the launch traced here: 75.2 us
  Pallas kernels  69.8 us (93%)
  local copies, waits for them, and re-layouts  3.16 us (4%)
  other arithmetic  1.58 us (2%)
    pallas_call x1, Pallas kernels, mixer(): pl.pallas_call(mixer_kernel, name='mixer', out_shape=(jax.ShapeDtypeStruc...  69.8 us
    unnamed x1, local copies, waits for them, and re-layouts  3.16 us
    transpose x1, other arithmetic, shards(): mixed = jnp.transpose(mixed.reshape(NQ, NS, 512).astype(BF16), (1, 0, 2))  1.58 us

profile of v3, /device:TPU:1, one launch (start us, length us, event | category | flops | bytes accessed | tf_op | source)
XLA Modules:
  0.0 75.2 jit_solution(18185375757705389016)
XLA Ops:
  0.6 69.8 %mixer.1 = (f32[96,512]{1,0:T(8,128)}, f32[8,512,128]{2,1,0:T(8,128)}) custom-call(bf16[12,8,4,8,128]{4,3,2,1,0:T(8,128)(2,1)} %bitcast.39, bf16[128,512]{1,0:T(8,128)(2,1)} %wx_h.1, bf16[128,512]{1,0:T(8,128)(2,1)} %wz_h.1, bf16[128,256]{1,0:T(8,128)(2,1)} %wb_h.1, bf16[128,256]{1,0:T(8,128)(2,1)} %wc_h.1, bf16[64,4096]{1,0:T(8,128)(2,1)} %bitcast.40, ...), custom_call_target="tpu_custom_call" | custom-call | tf_op jit(solution)/shard_map/mixer/pallas_call | solution.py:592
  70.5 1.6 %convert_bitcast_fusion = bf16[8,12,512]{2,0,1:T(8,128)(2,1)} fusion(f32[96,512]{1,0:T(8,128)} %get-tuple-element.4), kind=kLoop, calls=%fused_computation | loop fusion | flops 49152 | bytes 294912 | tf_op jit(solution)/shard_map/transpose | solution.py:716
  72.0 3.2 %copy.28 = f32[8,8,64,128]{3,2,1,0:T(8,128)} copy(f32[8,8,64,128]{3,2,1,0:T(8,128)} %bitcast.38) | data formatting | bytes 4194304

commit v4 on v3

v4 whole, which is shorter than its diff:
```python
import functools

import jax
import jax.numpy as jnp
from jax import lax
from jax.experimental import pallas as pl
from jax.experimental.pallas import tpu as pltpu
from jax.sharding import Mesh
from jax.sharding import PartitionSpec as P

NZ, NX, NY, NC = 8, 4, 4, 2
NT = NY * NC
MESH = pl.DeviceIdType.MESH
KV = ("z", "x")
TP = ("y", "c")
EPS = 1e-06
HIGH = lax.Precision.HIGHEST
F32 = jnp.float32
BF16 = jnp.bfloat16
NQ, NS, NP, NH = 12, 8, 6, 8
VMEM_LIMIT = 60 * 1024 * 1024


def wrap(i, n):
    return lax.rem(i + n, n)


def remote(src, dst, send_sem, recv_sem, device):
    return pltpu.make_async_remote_copy(
        src_ref=src,
        dst_ref=dst,
        send_sem=send_sem,
        recv_sem=recv_sem,
        device_id=device,
        device_id_type=MESH,
    )


def greet(devices):
    barrier = pltpu.get_barrier_semaphore()
    for device in devices:
        pl.semaphore_signal(barrier, inc=1, device_id=device, device_id_type=MESH)
    pl.semaphore_wait(barrier, len(devices))


def settle(view, sem):
    pltpu.make_async_copy(view, view, sem).wait()


def hops_of(piece, way):
    return 4 if (piece % 2 == 0) == (way == 0) else 3


def slot_of(piece, way, hop):
    return (0, 2, 4, 5)[hop - 1] if hops_of(piece, way) == 4 else (1, 3, 6)[hop - 1]


def sem_of(piece, way, hop):
    return hop - 1 if hop < hops_of(piece, way) else 3


def silu(v):
    return v * (1.0 / (1.0 + jnp.exp(-v)))


def softplus(v):
    return jnp.maximum(v, 0.0) + jnp.log1p(jnp.exp(-jnp.abs(v)))


def iota(shape, dim):
    return lax.broadcasted_iota(jnp.int32, shape, dim)


def dot(a, b):
    return jnp.dot(a.astype(BF16), b.astype(BF16), preferred_element_type=F32)


def dot_of(a, b, dims, precision=None):
    return lax.dot_general(
        a, b, ((dims[:1], dims[1:]), ((), ())), precision=precision, preferred_element_type=F32
    )


def past(first, last):
    return jnp.concatenate([first[...].astype(F32), last[...].astype(F32)], axis=0)


def widen(v):
    spread = (iota((NH, 512), 1) // 64 == iota((NH, 512), 0)).astype(F32)
    return dot_of(v, spread, (1, 0), HIGH)


def upright(row):
    wide = jnp.broadcast_to(row[...].astype(F32), (NS, NS))
    return jnp.sum(
        jnp.where(iota((NS, NS), 0) == iota((NS, NS), 1), wide, 0.0), axis=1, keepdims=True
    )


def mixer_kernel(
    tok_h,
    wx_h,
    wz_h,
    wb_h,
    wc_h,
    wdt_h,
    wo_h,
    state_h,
    gain,
    parents,
    accepted,
    cx,
    px,
    cb,
    pb,
    cc,
    pc,
    pdt,
    bias,
    alog,
    dskip,
    wtx,
    wtb,
    wtc,
    gain_out,
    mixed,
    new_state,
    tok,
    wown,
    wr,
    wo,
    held,
    fresh,
    tg,
    ts,
    wg,
    wog,
    prod,
    aprod,
    ring,
    aring,
    stage,
    astage,
    gated,
    gg,
    woc,
    kept,
    hold,
    given,
    taken,
    part,
    terms,
    l_s,
    s_s,
    n_s,
    t_s,
    t_r,
    f_r,
    w_s,
    w_r,
    r_s,
    a_s,
    r_r,
    o_s,
    o_r,
    g_s,
    g_r,
    d_s,
    d_r,
    p_s,
    p_r,
):
    z, x = lax.axis_index("z"), lax.axis_index("x")
    y, c = lax.axis_index("y"), lax.axis_index("c")
    t = y * NC + c
    count = NQ * NS

    def depth_of(owner):
        return pl.ds(pl.multiple_of(owner * 128, 128), 128)

    lower, upper = slice(0, 128), slice(128, 256)
    loads = [(tok_h, tok, 0), (wo_h, wo, 1)]
    loads.append(
        (
            wdt_h.at[
                pl.ds(pl.multiple_of(t * NH, NH), NH), pl.ds(pl.multiple_of(z * 512, 512), 512)
            ],
            wr,
            2,
        )
    )
    for g in range(2):
        wide, narrow = slice(256 * g, 256 * g + 256), slice(128 * g, 128 * g + 128)
        loads.append((wx_h.at[:, wide], wown.at[3 * g], 3 + g))
        loads.append((wb_h.at[:, narrow], wown.at[3 * g + 1, :, lower], 4))
        loads.append((wc_h.at[:, narrow], wown.at[3 * g + 1, :, upper], 4))
        loads.append((wz_h.at[:, wide], wown.at[3 * g + 2], 4))

    def load(k):
        return pltpu.make_async_copy(loads[k][0], loads[k][1], l_s.at[loads[k][2]])

    def load_state(s):
        return pltpu.make_async_copy(state_h.at[s], held.at[s], s_s.at[s // 4])

    def save_state(s):
        return pltpu.make_async_copy(held.at[s], new_state.at[s], n_s)

    for k in (3, 0, 1, 4, 5, 6, 2, 7, 8, 9, 10):
        load(k).start()
    for s in range(NS):
        load_state(s).start()
    plane = [(d, e) for d in range(NX) for e in range(NY) if d + e > 0]
    greet(
        [{"x": wrap(x + d, NX), "y": wrap(y + e, NY)} for d, e in plane]
        + [{"z": wrap(z + 1, NZ)}, {"z": wrap(z - 1, NZ)}, {"c": 1 - c}]
    )
    half = pl.ds(4 * c, 4)

    def tok_copy(d):
        to = wrap(x + d, NX)
        return remote(
            tok.at[:, half, to], tg.at[x, :, half], t_s, t_r.at[d - 1], {"x": to}
        )

    def tok_share(d):
        block = tg.at[wrap(x - d, NX), :, half]
        return remote(block, block, t_s, f_r.at[d - 1], {"c": 1 - c})

    def w_own(p, way):
        to = wrap(x + (1 if way == 0 else -1), NX)
        last = 0 if way == p % 2 else 1
        return remote(wown.at[p], wg.at[4 * p + x], w_s, w_r.at[p, last], {"x": to})

    def w_pass(p):
        sign = 1 if p % 2 == 0 else -1
        block = wg.at[4 * p + wrap(x - sign, NX)]
        return remote(block, block, w_s, w_r.at[p, 1], {"x": wrap(x + sign, NX)})

    def o_step(hop, side):
        for way in (0, 1):
            if hop == 4:
                side = way
            if hop == 4 or (hop > 1 and way == 0):
                settle(wog.at[0], o_r.at[2 * (hop - 2) + side])
            sign = 1 if way == 0 else -1
            owner = wrap(z - sign * (hop - 1), NZ)
            part = pl.ds(256 * side, 256)
            src = wo.at[part] if hop == 1 else wog.at[owner, part]
            to = {"z": wrap(z + sign, NZ)}
            at = 6 if hop == 4 else 2 * (hop - 1) + side
            sends.append(remote(src, wog.at[owner, part], o_s, o_r.at[at], to))
        for copy in sends[-2:]:
            copy.start()

    sends = []

    def r_copy(p, way, hop):
        to = {"z": wrap(z + (1 if way == 0 else -1), NZ)}
        buffer = aring if p == 6 else ring.at[p]
        dst = buffer.at[slot_of(p, way, hop)]
        if hop > 1:
            src = buffer.at[slot_of(p, way, hop - 1)]
        else:
            src = astage.at[way] if p == 6 else stage.at[p, way]
        return remote(src, dst, a_s if p == 6 else r_s, r_r.at[p, sem_of(p, way, hop)], to)

    def r_wait(p, index):
        buffer = aring if p == 6 else ring.at[p]
        first, many = ((0, 2), (2, 2), (4, 1), (5, 2))[index]
        settle(buffer.at[pl.ds(first, many)], r_r.at[p, index])

    def own_term(p, dest):
        if p == 6:
            return aprod[pl.ds(dest, 1)].reshape(16, count)
        return prod[p, :, pl.ds(dest, 1)].reshape(NQ, NS, 256)

    def r_step(p, hop):
        if hop > 1:
            r_wait(p, hop - 2)
        for way in (0, 1):
            hops = hops_of(p, way)
            if hop > hops:
                continue
            sign = 1 if way == 0 else -1
            term = own_term(p, wrap(z + sign * (hops + 1 - hop), NZ))
            if hop == 1:
                if p == 6:
                    astage[way] = term.astype(BF16)
                else:
                    stage[p, way] = term.astype(BF16)
            else:
                at = slot_of(p, way, hop - 1)
                if p == 6:
                    aring[at] = (aring[at].astype(F32) + term).astype(BF16)
                else:
                    ring[p, at] = (ring[p, at].astype(F32) + term).astype(BF16)
            r_copy(p, way, hop).start()

    def r_total(p):
        r_wait(p, 3)
        if p == 6:
            return own_term(p, z) + aring[5].astype(F32) + aring[6].astype(F32)
        total = own_term(p, z) + ring[p, 5].astype(F32) + ring[p, 6].astype(F32)
        return total.reshape(count, 256)

    order = (2, 1, 3)

    def w_send(p):
        w_own(p, p % 2).start()
        w_own(p, 1 - p % 2).start()

    load(3).wait()
    w_send(0)
    load(0).wait()
    for d in order:
        tok_copy(d).start()
    load(1).wait()
    o_step(1, 0)
    o_step(1, 1)

    up = jnp.concatenate([parents[:, q : q + 1] for q in range(NQ)], axis=0).astype(F32)
    taken_in = jnp.concatenate([upright(accepted)] * NQ, axis=0)
    seq = lax.rem(iota((count, 1), 0), NS).astype(F32)
    is_root = up < 0.0
    nodes = iota((count, 9 * NS + count), 1).astype(F32)

    def reach(back, other):
        return jnp.where(is_root, (taken_in + back) * NS + seq, other)

    at_kin = up * NS + seq
    kin = iota((count, count), 1).astype(F32)
    links = (kin == jnp.where(is_root, -1.0, at_kin)).astype(F32)
    eye = (iota((count, count), 0) == iota((count, count), 1)).astype(F32)
    family = eye + links
    for _ in range(4):
        family = jnp.minimum(dot(family, family), 1.0)
    is_kin = family > 0.5
    one = (nodes == reach(2.0, 9.0 * NS + at_kin)).astype(F32)
    two = dot(links, one) + (nodes == reach(1.0, -1.0)).astype(F32)
    three = dot(links, two) + (nodes == reach(0.0, -1.0)).astype(F32)
    one, two, three = one.astype(BF16), two.astype(BF16), three.astype(BF16)

    def window(history, taps):
        summed = taps[0:1] * history[0 : NP * NS]
        for k in (1, 2, 3):
            summed = summed + taps[k : k + 1] * history[k * NS : (k + NP) * NS]
        return silu(summed)

    rate = -jnp.exp(alog[...])
    path_xs = window(past(cx, px), wtx[...].astype(F32))
    path_bs = window(past(cb, pb), wtb[...].astype(F32))
    path_step = softplus(pdt[...].astype(F32) + bias[...])
    live = ((iota((NP * NS, 1), 0) // NS).astype(F32) < taken_in[0 : NP * NS]).astype(F32)
    path_log = path_step * rate * live
    tails = [jnp.zeros((NS, NH), F32)]
    for j in range(NP - 1, 0, -1):
        tails.insert(0, tails[0] + path_log[j * NS : (j + 1) * NS])
    overall = jnp.exp(tails[0] + path_log[0:NS])
    weights = live * jnp.exp(jnp.concatenate(tails, axis=0)) * path_step
    weighted = (path_xs * widen(weights)).astype(BF16)
    path_seq = lax.rem(iota((NP * NS, 128), 0), NS)

    def forward(p):
        settle(wg.at[0], w_r.at[p, 0])
        w_pass(p).start()

    forward(0)
    settle(wown.at[pl.ds(1, 5)], l_s.at[4])
    w_send(1)
    w_send(2)
    tg[pl.ds(x, 1)] = tok[:, :, pl.ds(x, 1)].reshape(1, NQ, NZ, NS, 128)
    for p in range(6):
        wg[pl.ds(4 * p + x, 1)] = wown[pl.ds(p, 1)]
    wog[pl.ds(z, 1)] = wo[...].reshape(1, 512, 128)
    load(2).wait()

    def rescale(d):
        xs = wrap(x - d, NX)
        values = tg[pl.ds(xs, 1)].reshape(NQ * NZ * NS, 128).astype(F32)
        scaled = (values * gain[pl.ds(z * NX + xs, 1), :]).astype(BF16)
        ts[:, :, :, depth_of(xs)] = scaled.reshape(NQ, NZ, NS, 128)
        return values * values

    squares = rescale(0)
    o_step(2, 0)

    gained = []
    for g in range(2):
        split_b = jnp.concatenate(
            [
                jnp.where(path_seq == s, path_bs[:, 128 * g : 128 * g + 128], 0.0)
                for s in range(NS)
            ],
            axis=1,
        ).astype(BF16)
        gained.append(dot_of(weighted[:, 256 * g : 256 * g + 256], split_b, (0, 0)))
    o_step(2, 1)
    for s in range(NS):
        if s % 4 == 0:
            settle(held.at[pl.ds(s, 4)], s_s.at[s // 4])
        at = slice(128 * s, 128 * s + 128)
        for g in range(2):
            wide = slice(256 * g, 256 * g + 256)
            fade = jnp.concatenate(
                [
                    jnp.broadcast_to(overall[s : s + 1, h : h + 1], (64, 128))
                    for h in range(4 * g, 4 * g + 4)
                ],
                axis=0,
            )
            now = fade * held[s, wide, :] + gained[g][:, at]
            held[s, wide, :] = now
            fresh[g, :, at] = now.astype(BF16)
        save_state(s).start()

    def tree_conv(history, own, taps):
        values = jnp.concatenate([history, own], axis=0).astype(BF16)
        summed = taps[3:4] * own
        for k, far in ((2, one), (1, two), (0, three)):
            summed = summed + taps[k : k + 1] * dot(far, values)
        return silu(summed)

    for d in order:
        settle(tg.at[0, :, half], t_r.at[d - 1])
        tok_share(d).start()
    o_step(3, 0)

    def multiply(p):
        settle(wg.at[pl.ds(0, 2)], w_r.at[p, 1])
        prod[p] = jnp.dot(
            ts[...].reshape(NQ * NZ * NS, 512),
            wg[4 * p : 4 * p + 4].reshape(512, 256),
            preferred_element_type=F32,
        ).reshape(NQ, NZ, NS, 256)
        r_step(p, 1)

    for d in order:
        if d == 3:
            forward(1)
            w_send(3)
        settle(tg.at[0, :, half], f_r.at[d - 1])
        squares = squares + rescale(d)
    multiply(0)
    o_step(3, 1)
    forward(2)
    w_send(4)
    multiply(1)
    forward(3)
    w_send(5)
    tall = jnp.concatenate([wr[...].astype(F32), jnp.zeros((8, 512), F32)], axis=0).astype(BF16)
    squares = squares.reshape(NQ, NZ, NS, 128)
    for dest in range(NZ):
        rates = dot_of(tall, ts[:, dest].reshape(count, 512), (1, 1))
        square = squares[:, dest].reshape(count, 128)
        above = square.astype(BF16)
        both = jnp.concatenate([above, (square - above.astype(F32)).astype(BF16)], axis=1)
        sums = dot_of(jnp.ones((16, 256), BF16), both, (1, 1))
        aprod[dest] = jnp.where(iota((16, count), 0) == NH, sums, rates)
    r_step(6, 1)
    r_step(0, 2)
    multiply(2)
    forward(4)
    r_step(1, 2)
    multiply(3)
    forward(5)
    o_step(4, 0)
    r_step(2, 2)
    r_step(6, 2)
    multiply(4)
    r_step(3, 2)
    multiply(5)
    r_step(0, 3)
    r_step(4, 2)
    r_step(6, 3)
    r_step(1, 3)
    r_step(5, 2)
    r_step(2, 3)
    settle(wog.at[0], o_r.at[6])
    for k in range(NZ):
        at = 512 * (k % 2) + 128 * (k // 2)
        woc[:, at : at + 128] = wog[k]
    r_step(3, 3)
    r_step(6, 4)
    r_step(4, 3)
    r_step(0, 4)
    r_step(5, 3)
    r_step(1, 4)
    r_step(2, 4)

    total = r_total(6)
    scale = lax.rsqrt(dot_of(eye, total, (1, 1), HIGH)[:, NH : NH + 1] / (NZ * NX * 128.0) + EPS)
    scale_t = lax.rsqrt(total[NH : NH + 1] / (NZ * NX * 128.0) + EPS)
    step_t = softplus((total[0:NH] * scale_t).astype(BF16).astype(F32) + upright(bias))
    slope_t = step_t * -jnp.exp(upright(alog))
    decay = dot_of(family, slope_t, (1, 1), HIGH)
    decay_t = dot_of(slope_t, family, (1, 1), HIGH)
    grown = widen(jnp.exp(decay))
    skip = widen(jnp.broadcast_to(dskip[...], (NS, NH)))[0:1]

    seq_of = lax.rem(iota((count, 128), 0), NS)
    side = iota((count, 128), 1)

    def scaled_rows(p):
        return (r_total(p) * scale).astype(BF16).astype(F32)

    def heads_of(g):
        wide, narrow = slice(256 * g, 256 * g + 256), slice(128 * g, 128 * g + 128)
        history = jnp.concatenate(
            [past(cx, px)[:, wide], past(cb, pb)[:, narrow], past(cc, pc)[:, narrow]], axis=1
        )
        taps = jnp.concatenate([wtx[:, wide], wtb[:, narrow], wtc[:, narrow]], axis=1)
        own = jnp.concatenate([scaled_rows(3 * g), scaled_rows(3 * g + 1)], axis=1)
        post = tree_conv(history, own, taps.astype(F32))
        post_b, post_c = post[:, 256:384].astype(BF16), post[:, 384:512].astype(BF16)
        post_x = post[:, 0:256].astype(BF16)
        split_c = jnp.concatenate(
            [jnp.where(seq_of == s, post_c.astype(F32), 0.0) for s in range(NS)], axis=1
        ).astype(BF16)
        carried = dot_of(split_c, fresh[g], (1, 1))
        scores = dot_of(post_c, post_b, (1, 1))
        within = []
        for pair in range(2):
            sides = []
            for h in (4 * g + 2 * pair, 4 * g + 2 * pair + 1):
                gap = decay[:, h : h + 1] - decay_t[h : h + 1, :]
                mixing = jnp.exp(jnp.where(is_kin, gap, 0.0)) * step_t[h : h + 1, :]
                mixing = jnp.where(is_kin, scores * mixing, 0.0)
                sides.append(dot(mixing, post_x[:, 128 * pair : 128 * pair + 128]))
            within.append(jnp.where(side < 64, sides[0], sides[1]))
        heads = carried * grown[:, wide] + jnp.concatenate(within, axis=1)
        return heads + skip[:, wide] * post[:, 0:256]

    def gate(g, heads):
        heads = heads * silu(scaled_rows(3 * g + 2))
        spread_of = jnp.sum(heads * heads, axis=1, keepdims=True) / 256.0
        heads = heads * lax.rsqrt(spread_of + EPS) * gain_out[:, 256 * g : 256 * g + 256]
        gated[g] = heads.astype(BF16)

    def g_copy(g, d):
        return remote(
            gated.at[g],
            gg.at[g, d - 1],
            g_s,
            g_r.at[0 if g == 0 else d],
            {"x": wrap(x + d, NX)},
        )

    def product(g, d, columns):
        values = gated[g] if d == 0 else gg[g, d - 1]
        return jnp.dot(
            values, woc[256 * g : 256 * g + 256, columns], preferred_element_type=F32
        )

    def d_copy(d):
        return remote(given.at[d], taken.at[d], d_s, d_r.at[d], {"c": 1 - c})

    def p_copy(d, e):
        to_y = wrap(y + e, NY)
        return remote(
            part.at[d, to_y],
            terms.at[x * NY + y],
            p_s,
            p_r,
            {"x": wrap(x - d, NX), "y": to_y},
        )

    mine = pl.ds(pl.multiple_of(512 * c, 512), 512)
    other = pl.ds(pl.multiple_of(512 * (1 - c), 512), 512)

    r_step(3, 4)
    r_step(4, 4)
    first = heads_of(0)
    r_step(5, 4)
    gate(0, first)
    for d in order:
        g_copy(0, d).start()
    gate(1, heads_of(1))
    for d in order:
        g_copy(1, d).start()
    def begin(d):
        hold[d] = product(0, d, other)
        kept[d] = product(0, d, mine)

    def finish(d):
        if d > 0:
            settle(gg.at[1, d - 1], g_r.at[d])
        given[d] = (hold[d] + product(1, d, other)).astype(BF16)
        d_copy(d).start()
        kept[d] = kept[d] + product(1, d, mine)

    def deliver(d):
        settle(taken.at[d], d_r.at[d])
        both = (kept[d] + taken[d].astype(F32)).astype(BF16)
        for to in range(NY):
            part[d, to] = both[:, 128 * to : 128 * to + 128]
        for e in (2, 1, 3, 0):
            if d + e > 0:
                p_copy(d, e).start()

    begin(0)
    finish(0)
    settle(gg.at[0], g_r.at[0])
    for d in order:
        begin(d)
    deliver(0)
    terms[pl.ds(x * NY + y, 1)] = part[0, pl.ds(y, 1)]
    finish(2)
    finish(1)
    deliver(2)
    finish(3)
    deliver(1)
    deliver(3)
    settle(terms.at[pl.ds(0, 15)], p_r)
    for xs in range(NX):
        total = terms[xs * NY].astype(F32)
        for k in range(1, NY):
            total = total + terms[xs * NY + k].astype(F32)
        mixed[:, xs * 128 : (xs + 1) * 128] = total.astype(BF16)

    settle(held, n_s)
    settle(wog.at[pl.ds(0, 7)], o_s)
    settle(tg.at[pl.ds(0, 3)], t_s)
    settle(wg.at[pl.ds(0, 18)], w_s)
    settle(ring, r_s)
    settle(aring, a_s)
    settle(gg, g_s)
    settle(given, d_s)
    settle(terms.at[pl.ds(0, 15)], p_s)


def mixer(*args):
    vmem = pl.BlockSpec(memory_space=pltpu.VMEM)
    far = pl.BlockSpec(memory_space=pl.ANY)
    dma = pltpu.SemaphoreType.DMA
    rows = NQ * NS
    return pl.pallas_call(
        mixer_kernel,
        name="mixer",
        out_shape=(
            jax.ShapeDtypeStruct((rows, 512), BF16),
            jax.ShapeDtypeStruct((NS, 512, 128), F32),
        ),
        in_specs=[far] * 8 + [vmem] * (len(args) - 8),
        out_specs=(vmem, far),
        scratch_shapes=[
            pltpu.VMEM((NQ, NZ, NX, NS, 128), BF16),
            pltpu.VMEM((6, 128, 256), BF16),
            pltpu.VMEM((NH, 512), BF16),
            pltpu.VMEM((512, 128), BF16),
            pltpu.VMEM((NS, 512, 128), F32),
            pltpu.VMEM((2, 256, 1024), BF16),
            pltpu.VMEM((NX, NQ, NZ, NS, 128), BF16),
            pltpu.VMEM((NQ, NZ, NS, 512), BF16),
            pltpu.VMEM((24, 128, 256), BF16),
            pltpu.VMEM((NZ, 512, 128), BF16),
            pltpu.VMEM((6, NQ, NZ, NS, 256), F32),
            pltpu.VMEM((NZ, 16, rows), F32),
            pltpu.VMEM((6, 7, NQ, NS, 256), BF16),
            pltpu.VMEM((7, 16, rows), BF16),
            pltpu.VMEM((6, 2, NQ, NS, 256), BF16),
            pltpu.VMEM((2, 16, rows), BF16),
            pltpu.VMEM((2, rows, 256), BF16),
            pltpu.VMEM((2, 3, rows, 256), BF16),
            pltpu.VMEM((512, 1024), BF16),
            pltpu.VMEM((NX, rows, 512), F32),
            pltpu.VMEM((NX, rows, 512), F32),
            pltpu.VMEM((NX, rows, 512), BF16),
            pltpu.VMEM((NX, rows, 512), BF16),
            pltpu.VMEM((NX, NY, rows, 128), BF16),
            pltpu.VMEM((NX * NY, rows, 128), BF16),
            dma((5,)),
            dma((2,)),
            dma,
            dma,
            dma((3,)),
            dma((3,)),
            dma,
            dma((6, 2)),
            dma,
            dma,
            dma((7, 4)),
            dma,
            dma((7,)),
            dma,
            dma((4,)),
            dma,
            dma((NX,)),
            dma,
            dma,
        ],
        compiler_params=pltpu.CompilerParams(
            collective_id=0, has_side_effects=True, vmem_limit_bytes=VMEM_LIMIT
        ),
    )(*args)


def finish_kernel(mixed_h, state_h, mixed_o, state_o, small, large, in_s, out_s):
    def steps(k):
        if k == NS:
            return mixed_h, small, mixed_o
        return state_h.at[k], large.at[k], state_o.at[k]

    def load(k):
        return pltpu.make_async_copy(steps(k)[0], steps(k)[1], in_s.at[k])

    def save(k):
        return pltpu.make_async_copy(steps(k)[1], steps(k)[2], out_s.at[k])

    for k in range(NS + 1):
        load(k).start()
    for k in range(NS + 1):
        load(k).wait()
        save(k).start()
    for k in range(NS + 1):
        save(k).wait()


def finish(mixed, new_state):
    far = pl.BlockSpec(memory_space=pltpu.HBM)
    return pl.pallas_call(
        finish_kernel,
        name="finish",
        out_shape=(
            jax.ShapeDtypeStruct(mixed.shape, mixed.dtype),
            jax.ShapeDtypeStruct(new_state.shape, new_state.dtype),
        ),
        in_specs=[far, far],
        out_specs=(far, far),
        scratch_shapes=[
            pltpu.VMEM(mixed.shape, mixed.dtype),
            pltpu.VMEM(new_state.shape, new_state.dtype),
            pltpu.SemaphoreType.DMA((NS + 1,)),
            pltpu.SemaphoreType.DMA((NS + 1,)),
        ],
        compiler_params=pltpu.CompilerParams(vmem_limit_bytes=VMEM_LIMIT),
    )(mixed, new_state)


def by_place(v):
    v = jnp.transpose(v, (1, 0, 2))
    return v.reshape(v.shape[0] * v.shape[1], v.shape[2])


def shards(
    tokens,
    parents,
    accepted,
    state,
    conv_x,
    conv_b,
    conv_c,
    path_x,
    path_b,
    path_c,
    path_dt,
    gain_in,
    w_x,
    w_z,
    w_b,
    w_c,
    w_dt,
    dt_bias,
    a_log,
    d_skip,
    conv_wx,
    conv_wb,
    conv_wc,
    gain_out,
    w_out,
):
    tok = jnp.transpose(tokens, (1, 0, 2)).reshape(NQ, NZ, NX, NS, 128)
    conv_x, path_x = by_place(conv_x), by_place(path_x)
    conv_b, path_b = by_place(conv_b), by_place(path_b)
    conv_c, path_c = by_place(conv_c), by_place(path_c)
    accepted, dt_bias, a_log = accepted[None, :], dt_bias[None, :], a_log[None, :]
    mixed, new_state = mixer(
        tok,
        w_x,
        w_z,
        w_b,
        w_c,
        w_dt.T,
        w_out,
        state.reshape(NS, 512, 128),
        gain_in.reshape(32, 128),
        parents,
        accepted,
        conv_x,
        path_x,
        conv_b,
        path_b,
        conv_c,
        path_c,
        by_place(path_dt),
        dt_bias,
        a_log,
        d_skip[None, :],
        conv_wx,
        conv_wb,
        conv_wc,
        gain_out[None, :],
    )
    mixed, new_state = finish(mixed, new_state)
    mixed = jnp.transpose(mixed.reshape(NQ, NS, 512), (1, 0, 2))
    return (mixed, new_state.reshape(NS, NH, 64, 128))


def solution(mesh):
    finer = Mesh(mesh.devices.reshape(NZ, NX, NY, NC), ("z", "x", "y", "c"))
    return jax.shard_map(
        shards,
        mesh=finer,
        in_specs=(
            P(None, None, KV),
            P(KV, None),
            P(KV),
            P(KV, TP, None, None),
            P(KV, None, TP),
            P(KV, None, TP),
            P(KV, None, TP),
            P(KV, None, TP),
            P(KV, None, TP),
            P(KV, None, TP),
            P(KV, None, TP),
            P(),
            P(KV, TP),
            P(KV, TP),
            P(KV, TP),
            P(KV, TP),
            P(),
            P(TP),
            P(TP),
            P(TP),
            P(None, TP),
            P(None, TP),
            P(None, TP),
            P(TP),
            P(TP, KV),
        ),
        out_specs=(P(KV, None, TP), P(KV, TP, None, None)),
        check_vma=False,
    )
```

time: 75.4 us -> 70.1 us (0.930)
  local copies, waits for them, and re-layouts: 3.16 us -> 0 us
  other arithmetic: 1.58 us -> 0 us
    unnamed x1 -> x0, local copies, waits for them, and re-layouts: 3.16 us -> none
    pallas_call x1, Pallas kernels: 69.8 us -> 66.9 us  [mixer(): pl.pallas_call(mixer_kernel, name='mixer', out_shape=(jax.ShapeDtypeStruc...]
    pallas_call x0 -> x1, Pallas kernels: none -> 2.44 us  [finish(): pl.pallas_call(finish_kernel, name='finish', out_shape=(jax.ShapeDtypeStr...]
    transpose x1 -> x0, other arithmetic: 1.58 us -> none  [shards(): mixed = jnp.transpose(mixed.reshape(NQ, NS, 512).astype(BF16), (1, 0, 2))]
where the time goes in v4:
time: 70.1 us; the launch traced here: 69.9 us
  Pallas kernels  69.3 us (99%)
    pallas_call x1, Pallas kernels, mixer(): pl.pallas_call(mixer_kernel, name='mixer', out_shape=(jax.ShapeDtypeStruc...  66.9 us
    pallas_call x1, Pallas kernels, finish(): pl.pallas_call(finish_kernel, name='finish', out_shape=(jax.ShapeDtypeStr...  2.44 us

profile of v4, /device:TPU:1, one launch (start us, length us, event | category | flops | bytes accessed | tf_op | source)
XLA Modules:
  0.0 69.9 jit_solution(5566769028819117289)
XLA Ops:
  0.6 66.9 %mixer.1 = (bf16[96,512]{1,0:T(8,128)(2,1)}, f32[8,512,128]{2,1,0:T(8,128)}) custom-call(bf16[12,8,4,8,128]{4,3,2,1,0:T(8,128)(2,1)} %bitcast.37, bf16[128,512]{1,0:T(8,128)(2,1)} %wx_h.1, bf16[128,512]{1,0:T(8,128)(2,1)} %wz_h.1, bf16[128,256]{1,0:T(8,128)(2,1)} %wb_h.1, bf16[128,256]{1,0:T(8,128)(2,1)} %wc_h.1, bf16[64,4096]{1,0:T(8,128)(2,1)} %bitcast.38, ...), custom_call_target="tpu_custom_call" | custom-call | tf_op jit(solution)/shard_map/mixer/pallas_call | solution.py:636
  67.5 2.4 %finish.1 = (bf16[96,512]{1,0:T(8,128)(2,1)}, f32[8,512,128]{2,1,0:T(8,128)}) custom-call(bf16[96,512]{1,0:T(8,128)(2,1)} %get-tuple-element.6.mixed_h, f32[8,512,128]{2,1,0:T(8,128)} %get-tuple-element.7.state_h), custom_call_target="tpu_custom_call" | custom-call | tf_op jit(solution)/shard_map/finish/pallas_call | solution.py:720

commit v5 on v4

--- a/solution.py
+++ b/solution.py
@@ -18,7 +18,7 @@
 F32 = jnp.float32
 BF16 = jnp.bfloat16
 NQ, NS, NP, NH = 12, 8, 6, 8
-VMEM_LIMIT = 60 * 1024 * 1024
+VMEM_LIMIT = 40 * 1024 * 1024
 
 
 def wrap(i, n):
@@ -152,7 +152,6 @@
     terms,
     l_s,
     s_s,
-    n_s,
     t_s,
     t_r,
     f_r,
@@ -201,9 +200,6 @@
 
     def load_state(s):
         return pltpu.make_async_copy(state_h.at[s], held.at[s], s_s.at[s // 4])
-
-    def save_state(s):
-        return pltpu.make_async_copy(held.at[s], new_state.at[s], n_s)
 
     for k in (3, 0, 1, 4, 5, 6, 2, 7, 8, 9, 10):
         load(k).start()
@@ -409,9 +405,8 @@
                 axis=0,
             )
             now = fade * held[s, wide, :] + gained[g][:, at]
-            held[s, wide, :] = now
+            new_state[s, wide, :] = now
             fresh[g, :, at] = now.astype(BF16)
-        save_state(s).start()
 
     def tree_conv(history, own, taps):
         values = jnp.concatenate([history, own], axis=0).astype(BF16)
@@ -423,7 +418,6 @@
     for d in order:
         settle(tg.at[0, :, half], t_r.at[d - 1])
         tok_share(d).start()
-    o_step(3, 0)
 
     def multiply(p):
         settle(wg.at[pl.ds(0, 2)], w_r.at[p, 1])
@@ -438,6 +432,7 @@
         if d == 3:
             forward(1)
             w_send(3)
+            o_step(3, 0)
         settle(tg.at[0, :, half], f_r.at[d - 1])
         squares = squares + rescale(d)
     multiply(0)
@@ -469,33 +464,23 @@
     multiply(4)
     r_step(3, 2)
     multiply(5)
+    r_step(6, 3)
     r_step(0, 3)
     r_step(4, 2)
-    r_step(6, 3)
     r_step(1, 3)
     r_step(5, 2)
+    r_step(6, 4)
     r_step(2, 3)
     settle(wog.at[0], o_r.at[6])
     for k in range(NZ):
         at = 512 * (k % 2) + 128 * (k // 2)
         woc[:, at : at + 128] = wog[k]
     r_step(3, 3)
-    r_step(6, 4)
     r_step(4, 3)
     r_step(0, 4)
     r_step(5, 3)
     r_step(1, 4)
     r_step(2, 4)
-
-    total = r_total(6)
-    scale = lax.rsqrt(dot_of(eye, total, (1, 1), HIGH)[:, NH : NH + 1] / (NZ * NX * 128.0) + EPS)
-    scale_t = lax.rsqrt(total[NH : NH + 1] / (NZ * NX * 128.0) + EPS)
-    step_t = softplus((total[0:NH] * scale_t).astype(BF16).astype(F32) + upright(bias))
-    slope_t = step_t * -jnp.exp(upright(alog))
-    decay = dot_of(family, slope_t, (1, 1), HIGH)
-    decay_t = dot_of(slope_t, family, (1, 1), HIGH)
-    grown = widen(jnp.exp(decay))
-    skip = widen(jnp.broadcast_to(dskip[...], (NS, NH)))[0:1]
 
     seq_of = lax.rem(iota((count, 128), 0), NS)
     side = iota((count, 128), 1)
@@ -569,6 +554,15 @@
 
     r_step(3, 4)
     r_step(4, 4)
+    total = r_total(6)
+    scale = lax.rsqrt(dot_of(eye, total, (1, 1), HIGH)[:, NH : NH + 1] / (NZ * NX * 128.0) + EPS)
+    scale_t = lax.rsqrt(total[NH : NH + 1] / (NZ * NX * 128.0) + EPS)
+    step_t = softplus((total[0:NH] * scale_t).astype(BF16).astype(F32) + upright(bias))
+    slope_t = step_t * -jnp.exp(upright(alog))
+    decay = dot_of(family, slope_t, (1, 1), HIGH)
+    decay_t = dot_of(slope_t, family, (1, 1), HIGH)
+    grown = widen(jnp.exp(decay))
+    skip = widen(jnp.broadcast_to(dskip[...], (NS, NH)))[0:1]
     first = heads_of(0)
     r_step(5, 4)
     gate(0, first)
@@ -617,7 +611,6 @@
             total = total + terms[xs * NY + k].astype(F32)
         mixed[:, xs * 128 : (xs + 1) * 128] = total.astype(BF16)
 
-    settle(held, n_s)
     settle(wog.at[pl.ds(0, 7)], o_s)
     settle(tg.at[pl.ds(0, 3)], t_s)
     settle(wg.at[pl.ds(0, 18)], w_s)
@@ -630,7 +623,7 @@
 
 def mixer(*args):
     vmem = pl.BlockSpec(memory_space=pltpu.VMEM)
-    far = pl.BlockSpec(memory_space=pl.ANY)
+    far = pl.BlockSpec(memory_space=pltpu.HBM)
     dma = pltpu.SemaphoreType.DMA
     rows = NQ * NS
     return pl.pallas_call(
@@ -641,7 +634,7 @@
             jax.ShapeDtypeStruct((NS, 512, 128), F32),
         ),
         in_specs=[far] * 8 + [vmem] * (len(args) - 8),
-        out_specs=(vmem, far),
+        out_specs=(vmem, vmem),
         scratch_shapes=[
             pltpu.VMEM((NQ, NZ, NX, NS, 128), BF16),
             pltpu.VMEM((6, 128, 256), BF16),
@@ -671,7 +664,6 @@
             dma((5,)),
             dma((2,)),
             dma,
-            dma,
             dma((3,)),
             dma((3,)),
             dma,
@@ -691,32 +683,24 @@
         compiler_params=pltpu.CompilerParams(
             collective_id=0, has_side_effects=True, vmem_limit_bytes=VMEM_LIMIT
         ),
-    )(*args)
-
-
-def finish_kernel(mixed_h, state_h, mixed_o, state_o, small, large, in_s, out_s):
-    def steps(k):
+    )(*(pltpu.with_memory_space_constraint(a, pltpu.HBM) for a in args))
+
+
+def finish_kernel(mixed, state, mixed_o, state_o, out_s):
+    def save(k):
         if k == NS:
-            return mixed_h, small, mixed_o
-        return state_h.at[k], large.at[k], state_o.at[k]
-
-    def load(k):
-        return pltpu.make_async_copy(steps(k)[0], steps(k)[1], in_s.at[k])
-
-    def save(k):
-        return pltpu.make_async_copy(steps(k)[1], steps(k)[2], out_s.at[k])
+            return pltpu.make_async_copy(mixed, mixed_o, out_s.at[1])
+        return pltpu.make_async_copy(state.at[k], state_o.at[k], out_s.at[0])
 
     for k in range(NS + 1):
-        load(k).start()
-    for k in range(NS + 1):
-        load(k).wait()
         save(k).start()
-    for k in range(NS + 1):
-        save(k).wait()
+    settle(state, out_s.at[0])
+    save(NS).wait()
 
 
 def finish(mixed, new_state):
     far = pl.BlockSpec(memory_space=pltpu.HBM)
+    near = pl.BlockSpec(memory_space=pltpu.VMEM)
     return pl.pallas_call(
         finish_kernel,
         name="finish",
@@ -724,15 +708,10 @@
             jax.ShapeDtypeStruct(mixed.shape, mixed.dtype),
             jax.ShapeDtypeStruct(new_state.shape, new_state.dtype),
         ),
-        in_specs=[far, far],
+        in_specs=[near, near],
         out_specs=(far, far),
-        scratch_shapes=[
-            pltpu.VMEM(mixed.shape, mixed.dtype),
-            pltpu.VMEM(new_state.shape, new_state.dtype),
-            pltpu.SemaphoreType.DMA((NS + 1,)),
-            pltpu.SemaphoreType.DMA((NS + 1,)),
-        ],
-        compiler_params=pltpu.CompilerParams(vmem_limit_bytes=VMEM_LIMIT),
+        scratch_shapes=[pltpu.SemaphoreType.DMA((2,))],
+        compiler_params=pltpu.CompilerParams(vmem_limit_bytes=8 * 1024 * 1024),
     )(mixed, new_state)
 
 

time: 70.1 us -> 68 us (0.970)
  Pallas kernels: 69.3 us -> 67.2 us
    pallas_call x1, Pallas kernels: 2.44 us -> 1.35 us  [finish(): pl.pallas_call(finish_kernel, name='finish', out_shape=(jax.ShapeDtypeStr...]
    pallas_call x1, Pallas kernels: 66.9 us -> 65.9 us  [mixer(): pl.pallas_call(mixer_kernel, name='mixer', out_shape=(jax.ShapeDtypeStruc...]
where the time goes in v5:
time: 68 us; the launch traced here: 67.9 us
  Pallas kernels  67.2 us (99%)
    pallas_call x1, Pallas kernels, mixer(): pl.pallas_call(mixer_kernel, name='mixer', out_shape=(jax.ShapeDtypeStruc...  65.9 us

profile of v5, /device:TPU:1, one launch (start us, length us, event | category | flops | bytes accessed | tf_op | source)
XLA Modules:
  0.0 67.9 jit_solution(17848272080187572718)
XLA Ops:
  0.6 65.9 %mixer.1 = (bf16[96,512]{1,0:T(8,128)(2,1)S(1)}, f32[8,512,128]{2,1,0:T(8,128)S(1)}) custom-call(bf16[12,8,4,8,128]{4,3,2,1,0:T(8,128)(2,1)} %bitcast.37, bf16[128,512]{1,0:T(8,128)(2,1)} %wx_h.1, bf16[128,512]{1,0:T(8,128)(2,1)} %wz_h.1, bf16[128,256]{1,0:T(8,128)(2,1)} %wb_h.1, bf16[128,256]{1,0:T(8,128)(2,1)} %wc_h.1, bf16[64,4096]{1,0:T(8,128)(2,1)} %bitcast.38, ...), custom_call_target="tpu_custom_call" | custom-call | tf_op jit(solution)/shard_map/mixer/pallas_call | solution.py:629
  66.5 1.3 %finish.1 = (bf16[96,512]{1,0:T(8,128)(2,1)}, f32[8,512,128]{2,1,0:T(8,128)}) custom-call(bf16[96,512]{1,0:T(8,128)(2,1)S(1)} %get-tuple-element.6.mixed, f32[8,512,128]{2,1,0:T(8,128)S(1)} %get-tuple-element.7.state), custom_call_target="tpu_custom_call" | custom-call | tf_op jit(solution)/shard_map/finish/pallas_call | solution.py:704

commit v6 on v5

--- a/solution.py
+++ b/solution.py
@@ -569,7 +569,7 @@
     for d in order:
         g_copy(0, d).start()
     gate(1, heads_of(1))
-    for d in order:
+    for d in (1, 3, 2):
         g_copy(1, d).start()
     def begin(d):
         hold[d] = product(0, d, other)
@@ -598,12 +598,12 @@
         begin(d)
     deliver(0)
     terms[pl.ds(x * NY + y, 1)] = part[0, pl.ds(y, 1)]
-    finish(2)
     finish(1)
-    deliver(2)
     finish(3)
     deliver(1)
+    finish(2)
     deliver(3)
+    deliver(2)
     settle(terms.at[pl.ds(0, 15)], p_r)
     for xs in range(NX):
         total = terms[xs * NY].astype(F32)

time: 68 us -> 68.4 us (level)
  no operation moved by 1% of the time
where the time goes in v6:
time: 68.4 us; the launch traced here: 68.2 us
  Pallas kernels  67.6 us (99%)
    pallas_call x1, Pallas kernels, mixer(): pl.pallas_call(mixer_kernel, name='mixer', out_shape=(jax.ShapeDtypeStruc...  66.3 us

profile of v6, /device:TPU:1, one launch (start us, length us, event | category | flops | bytes accessed | tf_op | source)
XLA Modules:
  0.0 68.2 jit_solution(3382102331094467595)
XLA Ops:
  0.6 66.3 %mixer.1 = (bf16[96,512]{1,0:T(8,128)(2,1)S(1)}, f32[8,512,128]{2,1,0:T(8,128)S(1)}) custom-call(bf16[12,8,4,8,128]{4,3,2,1,0:T(8,128)(2,1)} %bitcast.37, bf16[128,512]{1,0:T(8,128)(2,1)} %wx_h.1, bf16[128,512]{1,0:T(8,128)(2,1)} %wz_h.1, bf16[128,256]{1,0:T(8,128)(2,1)} %wb_h.1, bf16[128,256]{1,0:T(8,128)(2,1)} %wc_h.1, bf16[64,4096]{1,0:T(8,128)(2,1)} %bitcast.38, ...), custom_call_target="tpu_custom_call" | custom-call | tf_op jit(solution)/shard_map/mixer/pallas_call | solution.py:629
  66.9 1.3 %finish.1 = (bf16[96,512]{1,0:T(8,128)(2,1)}, f32[8,512,128]{2,1,0:T(8,128)}) custom-call(bf16[96,512]{1,0:T(8,128)(2,1)S(1)} %get-tuple-element.6.mixed, f32[8,512,128]{2,1,0:T(8,128)S(1)} %get-tuple-element.7.state), custom_call_target="tpu_custom_call" | custom-call | tf_op jit(solution)/shard_map/finish/pallas_call | solution.py:704

commit v7 on v6

--- a/solution.py
+++ b/solution.py
@@ -98,6 +98,7 @@
 
 
 def mixer_kernel(
+    fetches,
     tok_h,
     wx_h,
     wz_h,
@@ -203,6 +204,8 @@
 
     for k in (3, 0, 1, 4, 5, 6, 2, 7, 8, 9, 10):
         load(k).start()
+    for fetch in fetches:
+        fetch.start()
     for s in range(NS):
         load_state(s).start()
     plane = [(d, e) for d in range(NX) for e in range(NY) if d + e > 0]
@@ -210,6 +213,8 @@
         [{"x": wrap(x + d, NX), "y": wrap(y + e, NY)} for d, e in plane]
         + [{"z": wrap(z + 1, NZ)}, {"z": wrap(z - 1, NZ)}, {"c": 1 - c}]
     )
+    for fetch in fetches:
+        fetch.wait()
     half = pl.ds(4 * c, 4)
 
     def tok_copy(d):
@@ -601,8 +606,8 @@
     finish(1)
     finish(3)
     deliver(1)
+    deliver(3)
     finish(2)
-    deliver(3)
     deliver(2)
     settle(terms.at[pl.ds(0, 15)], p_r)
     for xs in range(NX):
@@ -625,15 +630,26 @@
     vmem = pl.BlockSpec(memory_space=pltpu.VMEM)
     far = pl.BlockSpec(memory_space=pltpu.HBM)
     dma = pltpu.SemaphoreType.DMA
+    small = args[8:]
+
+    def entry(*refs):
+        far_refs, rest = refs[8 : len(args)], refs[len(args) :]
+        near_refs, near_s = rest[-len(small) - 1 : -1], rest[-1]
+        fetches = [
+            pltpu.make_async_copy(f, n, near_s.at[k])
+            for k, (f, n) in enumerate(zip(far_refs, near_refs))
+        ]
+        mixer_kernel(fetches, *refs[:8], *near_refs, *rest[: -len(small) - 1])
+
     rows = NQ * NS
     return pl.pallas_call(
-        mixer_kernel,
+        entry,
         name="mixer",
         out_shape=(
             jax.ShapeDtypeStruct((rows, 512), BF16),
             jax.ShapeDtypeStruct((NS, 512, 128), F32),
         ),
-        in_specs=[far] * 8 + [vmem] * (len(args) - 8),
+        in_specs=[far] * len(args),
         out_specs=(vmem, vmem),
         scratch_shapes=[
             pltpu.VMEM((NQ, NZ, NX, NS, 128), BF16),
@@ -679,6 +695,8 @@
             dma((NX,)),
             dma,
             dma,
+            *[pltpu.VMEM(a.shape, a.dtype) for a in small],
+            dma((len(small),)),
         ],
         compiler_params=pltpu.CompilerParams(
             collective_id=0, has_side_effects=True, vmem_limit_bytes=VMEM_LIMIT

time: 68.4 us -> 67.2 us (0.982)
  Pallas kernels: 67.6 us -> 66.5 us
    pallas_call x1, Pallas kernels: 66.3 us -> 65.1 us  [mixer(): pl.pallas_call(entry, name='mixer', out_shape=(jax.ShapeDtypeStruct((rows...]
where the time goes in v7:
time: 67.2 us; the launch traced here: 67.1 us
  Pallas kernels  66.5 us (99%)
    pallas_call x1, Pallas kernels, mixer(): pl.pallas_call(entry, name='mixer', out_shape=(jax.ShapeDtypeStruct((rows...  65.1 us
    pallas_call x1, Pallas kernels, finish(): pl.pallas_call(finish_kernel, name='finish', out_shape=(jax.ShapeDtypeStr...  1.35 us

profile of v7, /device:TPU:1, one launch (start us, length us, event | category | flops | bytes accessed | tf_op | source)
XLA Modules:
  0.0 67.1 jit_solution(15642073409961064343)
XLA Ops:
  0.6 65.1 %mixer.1 = (bf16[96,512]{1,0:T(8,128)(2,1)S(1)}, f32[8,512,128]{2,1,0:T(8,128)S(1)}) custom-call(bf16[12,8,4,8,128]{4,3,2,1,0:T(8,128)(2,1)} %bitcast.37, bf16[128,512]{1,0:T(8,128)(2,1)} %refs_1_.1, bf16[128,512]{1,0:T(8,128)(2,1)} %refs_2_.1, bf16[128,256]{1,0:T(8,128)(2,1)} %refs_3_.1, bf16[128,256]{1,0:T(8,128)(2,1)} %refs_4_.1, ...), custom_call_target="tpu_custom_call" | custom-call | tf_op jit(solution)/shard_map/mixer/pallas_call | solution.py:645
  65.8 1.3 %finish.1 = (bf16[96,512]{1,0:T(8,128)(2,1)}, f32[8,512,128]{2,1,0:T(8,128)}) custom-call(bf16[96,512]{1,0:T(8,128)(2,1)S(1)} %get-tuple-element.6.mixed, f32[8,512,128]{2,1,0:T(8,128)S(1)} %get-tuple-element.7.state), custom_call_target="tpu_custom_call" | custom-call | tf_op jit(solution)/shard_map/finish/pallas_call | solution.py:722
